TPU v7x, 128 devices: a whole 4x4x4 slice. The times are simulated.
128 devices in a mesh: sp: 64 (over z, y, x), tp: 2 (over core).
Axes of the slice: x: 4, y: 4, z: 4, core: 2. Of those that a mesh axis runs over, the one named last changes fastest.
Arguments:
- projected_queries: bfloat16 [32768, 1024], P('sp', 'tp'), may hold values from -6 to 6
- projected_keys: bfloat16 [32768, 1024], P('sp', 'tp'), may hold values from -6 to 6
- projected_values: bfloat16 [32768, 1024], P('sp', 'tp'), may hold values from -6 to 6
- output_gate_values: bfloat16 [32768, 1024], P('sp', 'tp'), may hold values from -6 to 6
- write_strength_logits: bfloat16 [32768, 8], P('sp', 'tp'), may hold values from -6.5 to 3
- decay_input_logits: bfloat16 [32768, 8], P('sp', 'tp'), may hold values from -5 to 5
- head_rate_logarithm: float32 [8], P('tp'), may hold values from -8 to 2.3
- extra_log_decay: float32 [32768, 8], P('sp', 'tp'), may hold values from -0.7 to 0
- per_head_norm_gain: float32 [128], replicated, may hold values from 0.1 to 1.9
- output_matrix: bfloat16 [1024, 2048], replicated, may hold values from -0.1875 to 0.1875
- residual: bfloat16 [32768, 2048], P(('sp', 'tp')), may hold values from -6 to 6
- mixture_norm_gain: float32 [2048], replicated, may hold values from 0.1 to 1.9
- selected_expert_index: int32 [32768, 4], P(('sp', 'tp')), may hold values from 0 to 127, all different within a row; in each aligned block of 256 rows (0 to 255, 256 to 511, ...) at most 12 rows name the same one
- routing_weight: float32 [32768, 4], P(('sp', 'tp')), may hold values from 0.1 to 0.9
- routed_gate_weight: bfloat16 [128, 2048, 512], P(('sp', 'tp')), may hold values from -0.125 to 0.125
- routed_up_weight: bfloat16 [128, 2048, 512], P(('sp', 'tp')), may hold values from -0.125 to 0.125
- routed_down_weight: bfloat16 [128, 512, 2048], P(('sp', 'tp')), may hold values from -0.25 to 0.25
- common_gate_weight: bfloat16 [2048, 512], replicated, may hold values from -0.125 to 0.125
- common_up_weight: bfloat16 [2048, 512], replicated, may hold values from -0.125 to 0.125
- common_down_weight: bfloat16 [512, 2048], replicated, may hold values from -0.25 to 0.25
Outputs:
- block_out: bfloat16 [32768, 2048], P(('sp', 'tp'))
Inputs may be any that keep to these rules, and one draw needn't show every extreme that they name: `selected_expert_index`: each row names 4 different experts. Among the rows that one device holds, no expert is named more than 12 times.
All inputs are finite; a program needn't handle non-finite values.
Results may differ from a plain program's by a relative error of at most 0.008.
Values may be sent and summed in bfloat16 or wider, within the bound.
No kernel may reach another device: no remote copies, remote signals or barrier semaphores. Data moves between devices by JAX's collectives and lax.ppermute only.
A program may use at most 192 MiB of HBM per device.

v0:
```python
import functools

import jax
import jax.numpy as jnp
from jax import lax
from jax.experimental import pallas as pl
from jax.experimental.pallas import tpu as pltpu
from jax.sharding import Mesh
from jax.sharding import PartitionSpec as P

TOP_K = 4
HD = 128
BLOCK = 128
KEEP = 8
SP = ("sp_0", "sp_1", "sp_2")
SP_TP = ("sp_0", "sp_1", "sp_2", "tp")
EPS = 1e-06
F32 = jnp.float32
BF16 = jnp.bfloat16


def dot_nn(a, b):
    return lax.dot_general(a, b, (((1,), (0,)), ((), ())), preferred_element_type=F32)


def dot_nt(a, b):
    return lax.dot_general(a, b, (((1,), (1,)), ((), ())), preferred_element_type=F32)


def dot_tn(a, b):
    return lax.dot_general(a, b, (((0,), (0,)), ((), ())), preferred_element_type=F32)


def parts(x):
    high = x.astype(BF16)
    return high, (x - high.astype(F32)).astype(BF16)


def rows_of(*arrays):
    return jnp.concatenate(arrays, axis=0)


def cols_of(*arrays):
    return jnp.concatenate(arrays, axis=1)


def fine(a, b):
    ah, al = a
    bh, bl = b
    return dot_nn(cols_of(ah, al), rows_of(bh, bh)) + dot_nn(ah, bl)


def fine_square(a, b):
    ah, al = a
    bh, bl = b
    both = dot_nn(cols_of(ah, al), rows_of(cols_of(bh, bl), cols_of(bh, jnp.zeros_like(bl))))
    return both[:, :HD] + both[:, HD:]


def own_row(ref, head):
    table = ref[...].astype(F32)
    which = lax.broadcasted_iota(jnp.int32, table.shape, 0)
    return jnp.sum(jnp.where(which == head, table, 0.0), axis=0, keepdims=True)


def decay_sums(rate_ref, decay_ref, extra_ref, head):
    length = decay_ref.shape[1]
    raw = own_row(decay_ref, head) - 6.0
    soft = jnp.maximum(raw, 0.0) + jnp.log1p(jnp.exp(-jnp.abs(raw)))
    rate = jnp.exp(jnp.full((1, length), rate_ref[head], F32))
    total = jnp.broadcast_to(own_row(extra_ref, head) - rate * soft, (8, length))
    lane = lax.broadcasted_iota(jnp.int32, total.shape, 1)
    shift = 1
    while shift < length:
        total = total + jnp.where(lane >= shift, pltpu.roll(total, shift, 1), 0.0)
        shift *= 2
    g_row = total[0:1, :]
    return g_row, jnp.broadcast_to(g_row, (HD, length)).T


def unit(ref):
    x = ref[...].astype(F32)
    active = x * jax.nn.sigmoid(x)
    return active * lax.rsqrt(jnp.sum(active * active, axis=-1, keepdims=True) + EPS)


def against_keys(left, keys, number, g_row, g_col):
    ii = lax.broadcasted_iota(jnp.int32, (BLOCK, BLOCK), 0)
    jj = lax.broadcasted_iota(jnp.int32, (BLOCK, BLOCK), 1)
    blocks = []
    for r in range(number):
        here = slice(r * BLOCK, (r + 1) * BLOCK)
        upto = slice(0, (r + 1) * BLOCK)
        high = keys[0][upto]
        both = dot_nt(cols_of(left[0][here], left[1][here]), cols_of(high, high))
        both = both + dot_nt(left[0][here], keys[1][upto])
        row = []
        for c in range(r + 1):
            there = slice(c * BLOCK, (c + 1) * BLOCK)
            gap = g_col[here] - g_row[:, there]
            if c == r:
                gap = jnp.where(ii >= jj, gap, -1e30)
            row.append(both[:, there] * jnp.exp(gap))
        blocks.append(row)
    return blocks


def head_at(slots, step, place, heads):
    return (place + jnp.where(step == 0, slots[0], slots[1])) % heads


def maps_kernel(slots, place_ref, rate_ref, k_ref, v_ref, write_ref, decay_ref, extra_ref, *refs):
    one_ref, two_ref, high_ref, low_ref = refs[-4:]
    length = k_ref.shape[0]
    number = length // BLOCK
    step = pl.program_id(0)
    head = head_at(slots, step, place_ref[0], rate_ref.shape[0])
    g_row, g_col = decay_sums(rate_ref, decay_ref, extra_ref, head)
    beta = jax.nn.sigmoid(own_row(write_ref, head))
    b_col = jnp.broadcast_to(beta, (HD, length)).T
    keys = unit(k_ref)
    raw = v_ref[...].astype(F32)
    values = raw * jax.nn.sigmoid(raw)
    k_beta = keys * b_col
    right = cols_of(k_beta * jnp.exp(g_col), values * b_col)
    g_last = g_col[length - 1 : length, :]
    k_late = parts(keys * jnp.exp(g_last - g_col))
    lower = against_keys(parts(k_beta), parts(keys), number, g_row, g_col)
    ii = lax.broadcasted_iota(jnp.int32, (BLOCK, BLOCK), 0)
    jj = lax.broadcasted_iota(jnp.int32, (BLOCK, BLOCK), 1)
    eye = (ii == jj).astype(F32)
    near = (ii // 2 == jj // 2) & (ii > jj)
    inverse = [eye - jnp.where(near, lower[r][r], 0.0) for r in range(number)]

    def widen(level, inverse):
        chosen = (ii >> (level + 1) == jj >> (level + 1)) & (ii >> level > jj >> level)
        halves = [parts(t) for t in inverse]
        steps = [
            fine_square(halves[r], parts(jnp.where(chosen, lower[r][r], 0.0)))
            for r in range(number)
        ]
        return [inverse[r] - fine_square(parts(steps[r]), halves[r]) for r in range(number)]

    inverse = lax.fori_loop(1, BLOCK.bit_length() - 1, widen, inverse)
    highs, lows = [], []
    for r in range(number):
        here = slice(r * BLOCK, (r + 1) * BLOCK)
        rest = right[here]
        if r > 0:
            known = (rows_of(*highs), rows_of(*lows))
            rest = rest - fine(parts(cols_of(*lower[r][:r])), known)
        one = parts(fine(parts(inverse[r]), parts(rest)))
        highs.append(one[0])
        lows.append(one[1])
        high_ref[here, :] = one[0]
        low_ref[here, :] = one[1]
    high, low = rows_of(*highs), rows_of(*lows)
    moved = dot_tn(rows_of(*k_late), rows_of(high, high)) + dot_tn(k_late[0], low)
    whole = cols_of(eye * jnp.exp(g_last) - moved[:, :HD], moved[:, HD:])
    for k, map_ref in enumerate((one_ref, two_ref)):

        @pl.when(step == k)
        def _(map_ref=map_ref):
            map_ref[...] = whole


def mixes_kernel(rate_ref, q_ref, k_ref, decay_ref, extra_ref, high_ref, low_ref, qe_ref, o0_ref):
    length = q_ref.shape[0]
    number = length // BLOCK
    g_row, g_col = decay_sums(rate_ref, decay_ref, extra_ref, pl.program_id(0))
    queries = unit(q_ref)
    mixing = against_keys(parts(queries), parts(unit(k_ref)), number, g_row, g_col)
    grown = queries * jnp.exp(g_col)
    for r in range(number):
        here = slice(r * BLOCK, (r + 1) * BLOCK)
        upto = slice(0, (r + 1) * BLOCK)
        mixed = fine(parts(cols_of(*mixing[r])), (high_ref[upto, :], low_ref[upto, :]))
        qe_ref[here, :] = grown[here] - mixed[:, :HD]
        o0_ref[here, :] = mixed[:, HD:]


def state_maps(slots, keys, values, write_logits, decays, rates, place, filled):
    length, wide = keys.shape
    heads = wide // HD

    def whose(step, place_ref):
        return 0, head_at(slots, step, place_ref[0], heads)

    column = pl.BlockSpec((length, HD), whose)
    double = pl.BlockSpec((length, 2 * HD), whose)
    table = pl.BlockSpec((heads, length), lambda step, place_ref: (0, 0))
    small = pl.BlockSpec(memory_space=pltpu.SMEM)
    one_map = pl.BlockSpec((HD, 2 * HD), lambda step, place_ref: (0, 0))
    kept = [pl.BlockSpec(memory_space=pl.ANY)] * len(filled)
    return pl.pallas_call(
        functools.partial(maps_kernel, slots),
        grid_spec=pltpu.PrefetchScalarGridSpec(
            num_scalar_prefetch=1,
            grid=(2,),
            in_specs=[small, column, column, table, table, table] + kept,
            out_specs=[one_map, one_map, double, double],
        ),
        out_shape=[pltpu.VMEM((HD, 2 * HD), F32)] * 2
        + [jax.ShapeDtypeStruct((length, 2 * wide), BF16)] * 2,
        input_output_aliases={7: 2, 8: 3} if filled else {},
        name="maps",
    )(place, rates, keys, values, write_logits.T, *decays, *filled)


def mixes(queries, keys, decays, rates, high, low):
    length, wide = queries.shape
    heads = wide // HD
    column = pl.BlockSpec((length, HD), lambda h: (0, h))
    double = pl.BlockSpec((length, 2 * HD), lambda h: (0, h))
    table = pl.BlockSpec((heads, length), lambda h: (0, 0))
    small = pl.BlockSpec(memory_space=pltpu.SMEM)
    return pl.pallas_call(
        mixes_kernel,
        grid=(heads,),
        in_specs=[small, column, column, table, table, double, double],
        out_specs=[column, column],
        out_shape=[jax.ShapeDtypeStruct((length, wide), F32)] * 2,
        name="mixes",
    )(rates, queries, keys, *decays, high, low)


def shift_in(later):
    wide = lax.broadcasted_iota(jnp.int32, later.shape, 1)
    return jnp.where(wide >= HD, later, 0.0)


def then(later, earlier):
    return fine(parts(later[:, :HD]), parts(earlier)) + shift_in(later)


def identity_map():
    ii = lax.broadcasted_iota(jnp.int32, (HD, 2 * HD), 0)
    jj = lax.broadcasted_iota(jnp.int32, (HD, 2 * HD), 1)
    return (ii == jj).astype(F32)


def in_order(place, refs, held_ref):
    number = len(refs)
    for s, ref in enumerate(refs):
        held_ref[(place + number - s) % number] = ref[...]


def all_before_kernel(place_ref, *refs):
    maps, (before_ref, total_ref, held_ref) = refs[:-3], refs[-3:]
    in_order(place_ref[0], maps, held_ref)
    running = identity_map()
    for k in range(len(maps)):
        before_ref[k] = running
        running = held_ref[k] if k == 0 else then(held_ref[k], running)
    total_ref[...] = running


def mine_before_kernel(place_ref, *refs):
    maps, (before_ref, total_ref, held_ref) = refs[:-3], refs[-3:]
    place = place_ref[0]
    in_order(place, maps, held_ref)
    running = identity_map()
    before_ref[...] = running
    for k in range(len(maps)):
        running = held_ref[k] if k == 0 else then(held_ref[k], running)

        @pl.when(place == k + 1)
        def _(running=running):
            before_ref[...] = running

    total_ref[...] = running


def small_call(kernel, out_shape, scratch, place, *arrays):
    return pl.pallas_call(
        kernel,
        in_specs=[pl.BlockSpec(memory_space=pltpu.SMEM)]
        + [pl.BlockSpec(memory_space=pltpu.VMEM)] * len(arrays),
        out_shape=out_shape,
        scratch_shapes=scratch,
        compiler_params=pltpu.CompilerParams(vmem_limit_bytes=8 << 20),
    )(place, *[pltpu.with_memory_space_constraint(a, pltpu.VMEM) for a in arrays])


def states_kernel(place_ref, one_ref, two_ref, three_ref, middle_ref, inner_ref, *out_refs):
    state = three_ref[:, HD:]
    for ref in (two_ref, one_ref, middle_ref):
        state = fine(parts(ref[:, :HD]), parts(state)) + ref[:, HD:]
    pair = parts(state)
    number = len(out_refs)
    for s, out_ref in enumerate(out_refs):
        k = (place_ref[0] + number - s) % number
        out_ref[...] = fine(parts(inner_ref[k, :, :HD]), pair) + inner_ref[k, :, HD:]


def ring(array, axis, step):
    count = lax.axis_size(axis)
    return lax.ppermute(array, axis, [(i, (i + step) % count) for i in range(count)])


def onward(array, axis, step):
    count = lax.axis_size(axis)
    return lax.ppermute(array, axis, [(i, i + step) for i in range(count - step)])


def place_on(axis):
    return lax.axis_index(axis).reshape(1).astype(jnp.int32)


def entering(own, arrived, place):
    number = 1 + len(arrived)
    one = pltpu.VMEM(own.shape, F32)
    many = pltpu.VMEM((number,) + own.shape, F32)
    held = [pltpu.VMEM((number,) + own.shape, F32)]
    inner, line = small_call(all_before_kernel, [many, one], held, place, own, *arrived)
    two = ring(line, "sp_1", 2)
    first, three = [ring(line, "sp_1", s) for s in (1, 3)]
    middle, plane = small_call(
        mine_before_kernel, [one, one], held, place_on("sp_1"), line, first, two, three
    )
    two, first, three = [onward(plane, "sp_0", s) for s in (2, 1, 3)]
    found = small_call(
        states_kernel,
        [pltpu.VMEM((HD, HD), F32)] * number,
        (),
        place,
        first,
        two,
        three,
        middle,
        inner,
    )
    two, first, three = [ring(found[s], "sp_2", number - s) for s in (2, 1, 3)]
    return [found[0], first, two, three]


def finish_kernel(place_ref, core_ref, qe_ref, o0_ref, gate_ref, gain_ref, *refs):
    states, (keep_ref, send_ref, whole_ref) = refs[:-3], refs[-3:]
    number = len(states)
    half = keep_ref.shape[0]
    core = core_ref[0]

    @pl.loop(0, number)
    def _(h):
        there = pl.ds(pl.multiple_of(h * HD, HD), HD)
        slot = (h + number - place_ref[0]) % number
        state = states[0][...]
        for s in range(1, number):
            state = jnp.where(slot == s, states[s][...], state)
        mix = o0_ref[:, there] + fine(parts(qe_ref[:, there]), parts(state))
        scaled = mix * lax.rsqrt(jnp.mean(mix * mix, axis=-1, keepdims=True) + EPS)
        gate = gate_ref[:, there].astype(F32)
        whole_ref[...] = scaled * gain_ref[...] * (gate * jax.nn.sigmoid(gate))
        keep_ref[:, there] = whole_ref[pl.ds(core * half, half), :].astype(BF16)
        send_ref[:, there] = whole_ref[pl.ds((1 - core) * half, half), :].astype(BF16)


def finish(qe, o0, states, gate, gain, place):
    length, wide = qe.shape
    small = pl.BlockSpec(memory_space=pltpu.SMEM)
    arrays = (qe, o0, gate, gain.reshape(1, HD), *states)
    return pl.pallas_call(
        finish_kernel,
        in_specs=[small, small] + [pl.BlockSpec(memory_space=pltpu.VMEM)] * len(arrays),
        out_shape=[pltpu.VMEM((length // 2, wide), BF16)] * 2,
        scratch_shapes=[pltpu.VMEM((length, HD), F32)],
        compiler_params=pltpu.CompilerParams(vmem_limit_bytes=12 << 20),
        name="finish",
    )(
        place,
        place_on("tp"),
        *[pltpu.with_memory_space_constraint(a, pltpu.VMEM) for a in arrays],
    )


def feed_forward(rows, w_gate, w_up, w_down):
    hidden = jax.nn.silu(jnp.dot(rows, w_gate, preferred_element_type=F32))
    hidden = (hidden * jnp.dot(rows, w_up, preferred_element_type=F32)).astype(BF16)
    return jnp.dot(hidden, w_down, preferred_element_type=F32)


def exchange(rows):
    return lax.all_to_all(rows, SP_TP, split_axis=0, concat_axis=0, tiled=True)


def routes(index, weight, experts, room):
    length = index.shape[0]
    ids = jnp.arange(experts, dtype=jnp.int32)[:, None]
    named = jnp.zeros((experts, length), F32)
    weights = jnp.zeros((experts, length), F32)
    for j in range(index.shape[1]):
        here = index[:, j][None, :] == ids
        named = named + here.astype(F32)
        weights = weights + jnp.where(here, weight[:, j][None, :], 0.0)
    place = jnp.arange(length, dtype=jnp.int32)
    earlier = (place[:, None] < place[None, :]).astype(BF16)
    slot = jnp.dot(named.astype(BF16), earlier, preferred_element_type=F32)
    plain = jnp.where(named > 0, slot, -1.0)
    slot = plain[:, None, :]
    step = jnp.arange(KEEP, dtype=jnp.int32)[None, :, None]
    extra = room - KEEP
    first = slot == step.astype(F32)
    rest = slot == (KEEP + step % extra).astype(F32)
    lead = rest & (step < extra)
    tail = rest & (step >= extra)
    weights = weights[:, None, :]

    def flat(mask):
        return mask.reshape(experts * KEEP, length)

    back = [flat(jnp.where(m, weights, 0.0).astype(BF16)) for m in (first, lead, tail)]
    return plain, back


def places(slot_ref, start, count, length):
    slot = slot_ref[pl.ds(start, count), :]
    slot = jnp.broadcast_to(slot[:, None, :], (count, KEEP, length)).reshape(count * KEEP, length)
    step = lax.broadcasted_iota(jnp.int32, (count * KEEP, length), 0) % KEEP
    return slot, step


def attend_kernel(
    core_ref, keep_ref, came_ref, gain_ref, slot_ref, matrix_ref, residual_ref, *refs
):
    attended_ref, normed_ref, rest_ref, wide_ref, matrix_vmem, residual_vmem, done = refs
    length, dim = residual_ref.shape
    wide = keep_ref.shape[1]
    number = 4
    block = dim // number
    copies = [pltpu.make_async_copy(residual_ref, residual_vmem, done.at[number])]
    for c in range(number):
        there = pl.ds(c * block, block)
        copies.append(
            pltpu.make_async_copy(matrix_ref.at[:, there], matrix_vmem.at[:, there], done.at[c])
        )
    for copy in copies:
        copy.start()
    keep, came = keep_ref[...].astype(F32), came_ref[...].astype(F32)
    first_core = core_ref[0] == 0
    lead = jnp.where(first_core, keep, came).astype(BF16)
    tail = jnp.where(first_core, came, keep).astype(BF16)
    copies[0].wait()
    squares = jnp.zeros((length, 1), F32)
    for c in range(number):
        there = slice(c * block, (c + 1) * block)
        copies[1 + c].wait()
        projected = dot_nn(lead, matrix_vmem[:wide, there]) + dot_nn(tail, matrix_vmem[wide:, there])
        attended = (residual_vmem[:, there].astype(F32) + projected).astype(BF16)
        attended_ref[:, there] = attended
        plain = attended.astype(F32)
        wide_ref[:, there] = plain
        squares = squares + jnp.sum(plain * plain, axis=-1, keepdims=True)
    scale = lax.rsqrt(squares / dim + EPS)
    normed_ref[...] = (wide_ref[...] * scale * gain_ref[...]).astype(BF16)
    half = dim // 2
    count = 32

    @pl.loop(0, slot_ref.shape[0] // count)
    def _(i):
        start = pl.multiple_of(i * count, count)
        slot, step = places(slot_ref, start, count, length)
        extra = KEEP // 2
        chosen = slot == (KEEP + step % extra).astype(F32)
        lead = (chosen & (step < extra)).astype(F32).astype(BF16)
        tail = (chosen & (step >= extra)).astype(F32).astype(BF16)
        rows = dot_nn(lead, normed_ref[:, :half]) + dot_nn(tail, normed_ref[:, half:])
        rest_ref[pl.ds(start, count), :, :] = rows.astype(BF16).reshape(count, KEEP, half)


def attend(keep, came, out_matrix, residual, gain, slot):
    length, dim = residual.shape
    experts = slot.shape[0]
    arrays = (keep, came, gain.reshape(1, dim), slot)
    rows = pltpu.HBM((length, dim), BF16)
    return pl.pallas_call(
        attend_kernel,
        in_specs=[pl.BlockSpec(memory_space=pltpu.SMEM)]
        + [pl.BlockSpec(memory_space=pltpu.VMEM)] * len(arrays)
        + [pl.BlockSpec(memory_space=pl.ANY)] * 2,
        out_shape=[rows, rows, pltpu.HBM((experts, KEEP, dim // 2), BF16)],
        scratch_shapes=[
            pltpu.VMEM((length, dim), F32),
            pltpu.VMEM(out_matrix.shape, BF16),
            pltpu.VMEM((length, dim), BF16),
            pltpu.SemaphoreType.DMA((5,)),
        ],
        name="attend",
    )(
        place_on("tp"),
        *[pltpu.with_memory_space_constraint(a, pltpu.VMEM) for a in arrays],
        out_matrix,
        residual,
    )


def dispatch_kernel(slot_ref, normed_ref, out_ref):
    count, _, dim = out_ref.shape
    start = pl.multiple_of(pl.program_id(0) * count, count)
    slot, step = places(slot_ref, start, count, normed_ref.shape[0])
    chosen = (slot == step.astype(F32)).astype(F32).astype(BF16)
    rows = dot_nn(chosen, normed_ref[...]).astype(BF16)
    out_ref[...] = rows.reshape(count, KEEP, dim)


def dispatch(slot, normed):
    experts, length = slot.shape
    dim = normed.shape[1]
    count = 16
    return pl.pallas_call(
        dispatch_kernel,
        grid=(experts // count,),
        in_specs=[
            pl.BlockSpec((experts, length), lambda i: (0, 0)),
            pl.BlockSpec((length, dim), lambda i: (0, 0)),
        ],
        out_specs=pl.BlockSpec((count, KEEP, dim), lambda i: (i, 0, 0)),
        out_shape=jax.ShapeDtypeStruct((experts, KEEP, dim), BF16),
        name="dispatch",
    )(slot, normed)


def final_kernel(table_ref, rows_ref, early_ref, out_ref):
    out_ref[...] = (early_ref[...] + dot_nn(table_ref[...], rows_ref[...])).astype(BF16)


def final_sum(table, rows, early):
    length, wide = early.shape
    block = wide // 8
    column = pl.BlockSpec((length, block), lambda i: (0, i))
    return pl.pallas_call(
        final_kernel,
        grid=(wide // block,),
        in_specs=[
            pl.BlockSpec(table.shape, lambda i: (0, 0)),
            pl.BlockSpec((rows.shape[0], block), lambda i: (0, i)),
            column,
        ],
        out_specs=column,
        out_shape=jax.ShapeDtypeStruct((length, wide), BF16),
        name="final_sum",
    )(table, rows, early)


def shards(
    projected_queries,
    projected_keys,
    projected_values,
    output_gate_values,
    write_strength_logits,
    decay_input_logits,
    head_rate_logarithm,
    extra_log_decay,
    per_head_norm_gain,
    output_matrix,
    residual,
    mixture_norm_gain,
    selected_expert_index,
    routing_weight,
    routed_gate_weight,
    routed_up_weight,
    routed_down_weight,
    common_gate_weight,
    common_up_weight,
    common_down_weight,
):
    place = place_on("sp_2")
    decays = (decay_input_logits.T, extra_log_decay.T)
    base = (projected_keys, projected_values, write_strength_logits, decays, head_rate_logarithm)
    far, near, high, low = state_maps((2, 1), *base, place, ())
    far = ring(far, "sp_2", 2)
    near = ring(near, "sp_2", 1)
    last, own, high, low = state_maps((3, 0), *base, place, (high, low))
    states = entering(own, (near, far, ring(last, "sp_2", 3)), place)
    qe, o0 = mixes(projected_queries, projected_keys, decays, head_rate_logarithm, high, low)
    keep, send = finish(qe, o0, states, output_gate_values, per_head_norm_gain, place)
    came = ring(send, "tp", 1)
    length, dim = residual.shape
    experts = lax.axis_size(SP) * lax.axis_size("tp")
    room = max(2, length * TOP_K * 3 // (2 * experts))
    extra = room - KEEP
    half = dim // 2
    slot, (w_first, w_lead, w_tail) = routes(selected_expert_index, routing_weight, experts, room)
    attended, normed, rest_out = attend(
        keep, came, output_matrix, residual, mixture_norm_gain, slot
    )
    rest_in = exchange(rest_out)
    main_in = exchange(dispatch(slot, normed))
    shared = feed_forward(normed, common_gate_weight, common_up_weight, common_down_weight)

    weights = (routed_gate_weight[0], routed_up_weight[0], routed_down_weight[0])
    main_rows = feed_forward(main_in.reshape(experts * KEEP, dim), *weights).astype(BF16)
    main_back = exchange(main_rows.reshape(experts, KEEP, dim)).reshape(experts * KEEP, dim)
    unfolded = rest_in.reshape(experts, 2, extra, half).transpose(0, 2, 1, 3)
    rest_rows = feed_forward(unfolded.reshape(experts * extra, dim), *weights).astype(BF16)
    folded = rest_rows.reshape(experts, extra, 2, half).transpose(0, 2, 1, 3)
    rest_back = exchange(folded.reshape(experts, KEEP, half)).reshape(experts * KEEP, half)

    def combine(table, rows):
        return lax.dot_general(table, rows, (((0,), (0,)), ((), ())), preferred_element_type=F32)

    early = jnp.concatenate([combine(w_lead, rest_back), combine(w_tail, rest_back)], axis=1)
    early = early + attended.astype(F32) + shared
    return final_sum(w_first.T, main_back, early)


def solution(mesh):
    finer = Mesh(mesh.devices.reshape(4, 4, 4, mesh.shape["tp"]), ("sp_0", "sp_1", "sp_2", "tp"))
    in_specs = (
        P(SP, "tp"),
        P(SP, "tp"),
        P(SP, "tp"),
        P(SP, "tp"),
        P(SP, "tp"),
        P(SP, "tp"),
        P("tp"),
        P(SP, "tp"),
        P(),
        P(),
        P(SP_TP, None),
        P(),
        P(SP_TP, None),
        P(SP_TP, None),
        P(SP_TP, None, None),
        P(SP_TP, None, None),
        P(SP_TP, None, None),
        P(),
        P(),
        P(),
    )
    out_specs = P(SP_TP, None)

    return jax.shard_map(
        shards, mesh=finer, in_specs=in_specs, out_specs=out_specs, check_vma=False
    )
```

profile of v0, /device:TPU:1, one launch (start us, length us, event | category | flops | bytes accessed | tf_op | source)
XLA Modules:
  0.0 285.1 jit_solution(17420960643189318143)
XLA Ops:
  0.0 12.5 %maps.2 = (f32[128,256]{1,0:T(8,128)S(1)}, f32[128,256]{1,0:T(8,128)S(1)}, bf16[512,1024]{1,0:T(8,128)(2,1)}, bf16[512,1024]{1,0:T(8,128)(2,1)}) custom-call(s32[1]{0:T(128)} %bitcast.12.place_ref, f32[4]{0:T(128)} %rate_ref.5, bf16[512,512]{1,0:T(8,128)(2,1)} %k_ref.5, bf16[512,512]{1,0:T(8,128)(2,1)} %v_ref.3, bf16[4,512]{1,0:T(4,128)(2,1)} %bitcast.95, ...), custom_call_target="tpu_custom_call" | custom-call | tf_op jit(solution)/shard_map/maps/pallas_call | solution.py:195
  12.5 12.4 %maps.3 = (f32[128,256]{1,0:T(8,128)S(1)}, f32[128,256]{1,0:T(8,128)S(1)}, bf16[512,1024]{1,0:T(8,128)(2,1)}, bf16[512,1024]{1,0:T(8,128)(2,1)}) custom-call(s32[1]{0:T(128)} %bitcast.12.place_ref, f32[4]{0:T(128)} %rate_ref.5, bf16[512,512]{1,0:T(8,128)(2,1)} %k_ref.5, bf16[512,512]{1,0:T(8,128)(2,1)} %v_ref.3, ...), custom_call_target="tpu_custom_call", output_to_operand_aliasing={{2}: (7, {}), {3}: (8, {})} | custom-call | tf_op jit(solution)/shard_map/maps/pallas_call | solution.py:195
  24.9 3.3 %collective-permute-start.2 = (f32[128,256]{1,0:T(8,128)S(1)}, f32[128,256]{1,0:T(8,128)S(1)}, u32[]{:S(2)}, u32[]{:S(2)}) collective-permute-start(f32[128,256]{1,0:T(8,128)S(1)} %get-tuple-element.37), channel_id=1, source_target_pairs={{0,6},{2,0},{4,2},{6,4},{1,7},{3,1},{5,3},{7,5},{8,14},{10,8},{12,... | collective-permute-start | bytes 393224 | tf_op jit(solution)/shard_map/ppermute | solution.py:298
  28.1 1.7 collective-permute-start.1
  29.9 0.4 collective-permute-done.2.refs_3_
  30.3 5.0 %collective-permute-done.refs_1_ = f32[128,256]{1,0:T(8,128)S(1)} collective-permute-done((f32[128,256]{1,0:T(8,128)S(1)}, f32[128,256]{1,0:T(8,128)S(1)}, u32[]{:S(2)}, u32[]{:S(2)}) %collective-permute-start) | collective-permute-done | bytes 131104 | tf_op jit(solution)/shard_map/ppermute | solution.py:298
  35.3 0.6 shard_map.190
  35.9 1.4 collective-permute-start.3
  37.3 2.6 collective-permute-start.4
  39.9 1.1 collective-permute-start.5
  41.0 0.1 collective-permute-done.3.refs_1_
  41.1 2.7 collective-permute-done.4.refs_2_
  43.8 0.3 collective-permute-done.5.refs_3_
  44.1 0.7 shard_map.191
  44.7 3.6 %collective-permute-start.6 = (f32[128,256]{1,0:T(8,128)S(1)}, f32[128,256]{1,0:T(8,128)S(1)}, u32[]{:S(2)}, u32[]{:S(2)}) collective-permute-start(f32[128,256]{1,0:T(8,128)S(1)} %get-tuple-element.39), channel_id=1, source_target_pairs={{0,32},{32,64},{64,96},{1,33},{33,65},{65,97},{2,34},{34,66},{66,9... | collective-permute-start | bytes 393224 | tf_op jit(solution)/shard_map/ppermute | solution.py:303
  48.4 6.5 %collective-permute-start.7 = (f32[128,256]{1,0:T(8,128)S(1)}, f32[128,256]{1,0:T(8,128)S(1)}, u32[]{:S(2)}, u32[]{:S(2)}) collective-permute-start(f32[128,256]{1,0:T(8,128)S(1)} %get-tuple-element.39), channel_id=1, source_target_pairs={{0,64},{32,96},{1,65},{33,97},{2,66},{34,98},{3,67},{35,99},{4,68}... | collective-permute-start | bytes 393224 | tf_op jit(solution)/shard_map/ppermute | solution.py:303
  54.9 1.3 collective-permute-start.8
  56.3 0.6 collective-permute-done.7.two_ref
  56.9 2.7 collective-permute-done.8.three_ref
  59.5 0.8 shard_map.192
  60.3 1.0 collective-permute-start.10
  61.4 2.7 collective-permute-start.9
  64.1 7.1 %mixes.1 = (f32[512,512]{1,0:T(8,128)}, f32[512,512]{1,0:T(8,128)}) custom-call(f32[4]{0:T(128)} %rate_ref.5, bf16[512,512]{1,0:T(8,128)(2,1)} %q_ref.1, bf16[512,512]{1,0:T(8,128)(2,1)} %k_ref.5, bf16[4,512]{1,0:T(4,128)(2,1)} %bitcast.94, f32[4,512]{1,0:T(4,128)} %bitcast.91, bf16[512,1024]{1,0:T(8,128)(2,1)} %get-tuple-element.30.high_ref, ...), custom_call_target="tpu_custom_call" | custom-call | tf_op jit(solution)/shard_map/mixes/pallas_call | solution.py:217
  71.2 1.2 copy-done.4
  72.4 1.2 copy-done.5
  73.6 1.5 finish.1
  75.2 3.2 %collective-permute-start.12 = (bf16[256,512]{1,0:T(8,128)(2,1)S(1)}, bf16[256,512]{1,0:T(8,128)(2,1)S(1)}, u32[]{:S(2)}, u32[]{:S(2)}) collective-permute-start(bf16[256,512]{1,0:T(8,128)(2,1)S(1)} %get-tuple-element.47), channel_id=1, source_target_pairs={{0,1},{1,0},{2,3},{3,2},{4,5},{5,4},{6,7},{7,6},{8,9},{9,8},{10,11... | collective-permute-start | bytes 786440 | tf_op jit(solution)/shard_map/ppermute | solution.py:298
  78.4 0.2 convolution_select_fusion.slot_ref
  78.6 0.0 copy-start.2
  78.6 0.9 collective-permute-done.12.came_ref
  79.5 7.4 %attend.1 = (bf16[256,2048]{1,0:T(8,128)(2,1)}, bf16[256,2048]{1,0:T(8,128)(2,1)}, bf16[128,8,1024]{2,1,0:T(8,128)(2,1)}) custom-call(s32[1]{0:T(128)} %bitcast.11.core_ref, bf16[256,512]{1,0:T(8,128)(2,1)S(1)} %get-tuple-element.46.keep_ref, bf16[256,512]{1,0:T(8,128)(2,1)S(1)} %collective-permute-done.12.came_ref, f32[1,2048]{1,0:T(1,128)S(1)} %bitcast.83, ...), custom_call_target="tpu_custom_call" | custom-call | tf_op jit(solution)/shard_map/attend/pallas_call | solution.py:475
  86.9 8.2 %all-to-all-start.2 = ((bf16[128,8,1024]{2,1,0:T(8,128)(2,1)}), bf16[128,8,1024]{2,1,0:T(8,128)(2,1)}, u32[]{:S(2)}, u32[]{:S(2)}) async-start(bf16[128,8,1024]{2,1,0:T(8,128)(2,1)} %get-tuple-element.49), calls=%async_computation.2 | async-start | bytes 4194304 | tf_op jit(solution)/shard_map/all_to_all | solution.py:383
  95.2 6.2 %dispatch.1 = bf16[128,8,2048]{2,1,0:T(8,128)(2,1)} custom-call(f32[128,256]{1,0:T(8,128)} %copy-done.2, bf16[256,2048]{1,0:T(8,128)(2,1)} %get-tuple-element.48.normed_ref), custom_call_target="tpu_custom_call" | custom-call | tf_op jit(solution)/shard_map/dispatch/pallas_call | solution.py:509
  101.3 23.9 %all-to-all-done.2 = bf16[128,8,1024]{2,1,0:T(8,128)(2,1)} async-done(((bf16[128,8,1024]{2,1,0:T(8,128)(2,1)}), bf16[128,8,1024]{2,1,0:T(8,128)(2,1)}, u32[]{:S(2)}, u32[]{:S(2)}) %all-to-all-start.2) | async-done | bytes 2097184 | tf_op jit(solution)/shard_map/all_to_all | solution.py:383
  125.3 5.5 %all-to-all-start = ((bf16[128,8,2048]{2,1,0:T(8,128)(2,1)}), bf16[128,8,2048]{2,1,0:T(8,128)(2,1)}, u32[]{:S(2)}, u32[]{:S(2)}) async-start(bf16[128,8,2048]{2,1,0:T(8,128)(2,1)} %dispatch.1), calls=%async_computation | async-start | bytes 8388608 | tf_op jit(solution)/shard_map/all_to_all | solution.py:383
  130.8 0.1 select_add_fusion
  130.9 0.9 broadcast_bitcast_fusion
  131.8 0.1 broadcast_bitcast_fusion.1
  131.9 4.1 %reshape.230 = bf16[128,2,4,1024]{3,2,1,0:T(4,128)(2,1)} reshape(bf16[128,8,1024]{2,1,0:T(8,128)(2,1)} %all-to-all-done.2) | data formatting | bytes 4194304 | tf_op jit(solution)/shard_map/reshape | solution.py:593
  136.0 4.0 %copy.36 = bf16[128,2,4,1024]{3,1,2,0:T(2,128)(2,1)S(1)} copy(bf16[128,2,4,1024]{3,2,1,0:T(4,128)(2,1)} %reshape.230) | data formatting | bytes 4194304 | tf_op jit(solution)/shard_map/reshape | solution.py:593
  140.0 0.0 copy-start.13
  140.0 0.6 copy.38
  140.6 1.4 copy-done.9
  142.0 2.2 fusion.10
  144.2 6.2 %convolution_convert_fusion = bf16[512,2048]{1,0:T(8,128)(2,1)} fusion(bf16[1,512,2048]{2,1,0:T(8,128)(2,1)S(1)} %copy-done, bf16[512,2048]{1,0:T(8,128)(2,1)} %bitcast.88, bf16[1,2048,512]{2,1,0:T(8,128)(2,1)} %param.35, f32[512,512]{1,0:T(8,128)} %fusion.10), kind=kOutput, calls=%fused_computation.5 | convolution fusion | flops 2150105088 | bytes 9437184 | tf_op jit(solution)/shard_map/dot_general | solution.py:379
  150.5 4.5 %reshape.232 = bf16[128,4,2,1024]{3,2,1,0:T(2,128)(2,1)} reshape(bf16[512,2048]{1,0:T(8,128)(2,1)} %convolution_convert_fusion) | data formatting | bytes 4194304 | tf_op jit(solution)/shard_map/reshape | solution.py:595
  155.0 4.1 %copy.37 = bf16[128,2,4,1024]{3,2,1,0:T(4,128)(2,1)} copy(bf16[128,2,4,1024]{3,1,2,0:T(2,128)(2,1)} %bitcast.86) | data formatting | bytes 4194304 | tf_op jit(solution)/shard_map/transpose | solution.py:595
  159.1 4.0 %reshape.233 = bf16[128,8,1024]{2,1,0:T(8,128)(2,1)} reshape(bf16[128,2,4,1024]{3,2,1,0:T(4,128)(2,1)} %copy.37) | data formatting | bytes 4194304 | tf_op jit(solution)/shard_map/reshape | solution.py:596
  163.0 20.5 %all-to-all-done = bf16[128,8,2048]{2,1,0:T(8,128)(2,1)} async-done(((bf16[128,8,2048]{2,1,0:T(8,128)(2,1)}), bf16[128,8,2048]{2,1,0:T(8,128)(2,1)}, u32[]{:S(2)}, u32[]{:S(2)}) %all-to-all-start) | async-done | bytes 4194336 | tf_op jit(solution)/shard_map/all_to_all | solution.py:383
  183.5 5.5 %all-to-all-start.3 = ((bf16[128,8,1024]{2,1,0:T(8,128)(2,1)}), bf16[128,8,1024]{2,1,0:T(8,128)(2,1)}, u32[]{:S(2)}, u32[]{:S(2)}) async-start(bf16[128,8,1024]{2,1,0:T(8,128)(2,1)} %reshape.233), calls=%async_computation.3 | async-start | bytes 4194304 | tf_op jit(solution)/shard_map/all_to_all | solution.py:383
  189.0 2.1 copy.35
  191.1 1.3 copy.34
  192.4 0.1 eq.128
  192.5 2.5 fusion.30.table_ref
  195.0 5.8 %fusion.2 = f32[1024,512]{1,0:T(8,128)} fusion(bf16[128,8,2048]{2,1,0:T(8,128)(2,1)} %all-to-all-done, bf16[1,2048,512]{2,1,0:T(8,128)(2,1)S(1)} %copy-done.14), kind=kOutput, calls=%fused_computation.2 | convolution fusion | flops 2147483648 | bytes 8388608 | tf_op jit(solution)/shard_map/dot_general | solution.py:377
  200.8 10.0 %convert_bitcast_fusion = bf16[128,8,2048]{2,1,0:T(8,128)(2,1)} fusion(bf16[1,512,2048]{2,1,0:T(8,128)(2,1)S(1)} %copy-done, f32[1024,512]{1,0:T(8,128)} %fusion.2, bf16[1,2048,512]{2,1,0:T(8,128)(2,1)} %param.35, bf16[128,8,2048]{2,1,0:T(8,128)(2,1)} %all-to-all-done), kind=kOutput, calls=%fused_computation.4 | convolution fusion | flops 4300210176 | bytes 14680064 | tf_op jit(solution)/shard_map/dot_general | solution.py:379
  210.8 8.4 %all-to-all-done.3 = bf16[128,8,1024]{2,1,0:T(8,128)(2,1)} async-done(((bf16[128,8,1024]{2,1,0:T(8,128)(2,1)}), bf16[128,8,1024]{2,1,0:T(8,128)(2,1)}, u32[]{:S(2)}, u32[]{:S(2)}) %all-to-all-start.3) | async-done | bytes 2097184 | tf_op jit(solution)/shard_map/all_to_all | solution.py:383
  219.2 5.5 %all-to-all-start.1 = ((bf16[128,8,2048]{2,1,0:T(8,128)(2,1)}), bf16[128,8,2048]{2,1,0:T(8,128)(2,1)}, u32[]{:S(2)}, u32[]{:S(2)}) async-start(bf16[128,8,2048]{2,1,0:T(8,128)(2,1)} %convert_bitcast_fusion), calls=%async_computation.1 | async-start | bytes 8388608 | tf_op jit(solution)/shard_map/all_to_all | solution.py:383
  224.8 2.3 fusion.62
  227.1 3.5 %convolution_bitcast_fusion.1 = f32[256,1024]{1,0:T(8,128)} fusion(bf16[128,8,1024]{2,1,0:T(8,128)(2,1)} %all-to-all-done.3, bf16[128,256]{1,0:T(8,128)(2,1)S(1)} %select_add_fusion, f32[128,256]{1,0:T(8,128)S(1)} %copy-done.3, f32[8]{0:T(128)S(1)} %fusion.52, pred[8]{0:T(512)(128)(4,1)S(1)} %iota_compare_fusion.7), kind=kOutput, calls=%fused_computation.18 | convolution fusion | flops 537657344 | bytes 3342376 | tf_op jit(solution)/shard_map/dot_general | solution.py:599
  230.6 3.6 %convolution_bitcast_fusion = f32[256,1024]{1,0:T(8,128)} fusion(bf16[128,8,1024]{2,1,0:T(8,128)(2,1)} %all-to-all-done.3, bf16[128,256]{1,0:T(8,128)(2,1)S(1)} %select_add_fusion, f32[128,256]{1,0:T(8,128)S(1)} %copy-done.3, f32[8]{0:T(128)S(1)} %fusion.52, pred[8]{0:T(512)(128)(4,1)S(1)} %iota_compare_fusion.6), kind=kOutput, calls=%fused_computation.17 | convolution fusion | flops 537657344 | bytes 3342376 | tf_op jit(solution)/shard_map/dot_general | solution.py:599
  234.1 5.5 %fusion.4.early_ref = f32[256,2048]{1,0:T(8,128)} fusion(f32[256,1024]{1,0:T(8,128)} %convolution_bitcast_fusion, f32[256,1024]{1,0:T(8,128)} %convolution_bitcast_fusion.1, bf16[256,2048]{1,0:T(8,128)(2,1)S(1)} %copy-done.15, bf16[512,2048]{1,0:T(8,128)(2,1)} %param.39, f32[256,512]{1,0:T(8,128)S(1)} %fusion.62, bf16[256,2048]{1,0:T(8,128)(2,1)S(1)} %copy-done.10, ...), kind=kOutput, calls=%fused_computation.7 | convolution fusion | flops 1076625408 | bytes 11010048 | tf_op jit(solution)/shard_map/dot_general | solution.py:379
  239.6 37.9 %all-to-all-done.1 = bf16[128,8,2048]{2,1,0:T(8,128)(2,1)} async-done(((bf16[128,8,2048]{2,1,0:T(8,128)(2,1)}), bf16[128,8,2048]{2,1,0:T(8,128)(2,1)}, u32[]{:S(2)}, u32[]{:S(2)}) %all-to-all-start.1) | async-done | bytes 4194336 | tf_op jit(solution)/shard_map/all_to_all | solution.py:383
  277.5 7.6 %final_sum.1 = bf16[256,2048]{1,0:T(8,128)(2,1)} custom-call(bf16[256,1024]{1,0:T(8,128)(2,1)} %fusion.30.table_ref, bf16[1024,2048]{1,0:T(8,128)(2,1)} %bitcast.24.rows_ref, f32[256,2048]{1,0:T(8,128)} %fusion.4.early_ref), custom_call_target="tpu_custom_call" | custom-call | tf_op jit(solution)/shard_map/final_sum/pallas_call | solution.py:530
  (41 shorter events, 0.1 us)
Async XLA Ops:
  0.0 144.2 %copy-start = (bf16[1,512,2048]{2,1,0:T(8,128)(2,1)S(1)}, bf16[1,512,2048]{2,1,0:T(8,128)(2,1)}, u32[]{:S(2)}) copy-start(bf16[1,512,2048]{2,1,0:T(8,128)(2,1)} %param.36) | copy-start | bytes 6291460
  24.9 5.5 %collective-permute-start.2 = (f32[128,256]{1,0:T(8,128)S(1)}, f32[128,256]{1,0:T(8,128)S(1)}, u32[]{:S(2)}, u32[]{:S(2)}) collective-permute-start(f32[128,256]{1,0:T(8,128)S(1)} %get-tuple-element.37), channel_id=1, source_target_pairs={{0,6},{2,0},{4,2},{6,4},{1,7},{3,1},{5,3},{7,5},{8,14},{10,8},{12,... | collective-permute-start | bytes 393224 | tf_op jit(solution)/shard_map/ppermute | solution.py:298
  28.1 7.2 %collective-permute-start = (f32[128,256]{1,0:T(8,128)S(1)}, f32[128,256]{1,0:T(8,128)S(1)}, u32[]{:S(2)}, u32[]{:S(2)}) collective-permute-start(f32[128,256]{1,0:T(8,128)S(1)} %get-tuple-element.35), channel_id=1, source_target_pairs={{0,2},{2,4},{4,6},{6,0},{1,3},{3,5},{5,7},{7,1},{8,10},{10,12},{12... | collective-permute-start | bytes 393224 | tf_op jit(solution)/shard_map/ppermute | solution.py:298
  28.1 7.2 %collective-permute-start.1 = (f32[128,256]{1,0:T(8,128)S(1)}, f32[128,256]{1,0:T(8,128)S(1)}, u32[]{:S(2)}, u32[]{:S(2)}) collective-permute-start(f32[128,256]{1,0:T(8,128)S(1)} %get-tuple-element.36), channel_id=1, source_target_pairs={{0,4},{2,6},{4,0},{6,2},{1,5},{3,7},{5,1},{7,3},{8,12},{10,14},{12... | collective-permute-start | bytes 393224 | tf_op jit(solution)/shard_map/ppermute | solution.py:298
  35.9 5.2 %collective-permute-start.3 = (f32[128,256]{1,0:T(8,128)S(1)}, f32[128,256]{1,0:T(8,128)S(1)}, u32[]{:S(2)}, u32[]{:S(2)}) collective-permute-start(f32[128,256]{1,0:T(8,128)S(1)} %get-tuple-element.38.refs_0_), channel_id=1, source_target_pairs={{0,8},{8,16},{16,24},{24,0},{1,9},{9,17},{17,25},{25,1},{2,10},{10... | collective-permute-start | bytes 393224 | tf_op jit(solution)/shard_map/ppermute | solution.py:298
  37.3 6.5 %collective-permute-start.4 = (f32[128,256]{1,0:T(8,128)S(1)}, f32[128,256]{1,0:T(8,128)S(1)}, u32[]{:S(2)}, u32[]{:S(2)}) collective-permute-start(f32[128,256]{1,0:T(8,128)S(1)} %get-tuple-element.38.refs_0_), channel_id=1, source_target_pairs={{0,16},{8,24},{16,0},{24,8},{1,17},{9,25},{17,1},{25,9},{2,18},{10... | collective-permute-start | bytes 393224 | tf_op jit(solution)/shard_map/ppermute | solution.py:298
  39.9 4.2 %collective-permute-start.5 = (f32[128,256]{1,0:T(8,128)S(1)}, f32[128,256]{1,0:T(8,128)S(1)}, u32[]{:S(2)}, u32[]{:S(2)}) collective-permute-start(f32[128,256]{1,0:T(8,128)S(1)} %get-tuple-element.38.refs_0_), channel_id=1, source_target_pairs={{0,24},{8,0},{16,8},{24,16},{1,25},{9,1},{17,9},{25,17},{2,26},{10... | collective-permute-start | bytes 393224 | tf_op jit(solution)/shard_map/ppermute | solution.py:298
  44.7 11.5 %collective-permute-start.6 = (f32[128,256]{1,0:T(8,128)S(1)}, f32[128,256]{1,0:T(8,128)S(1)}, u32[]{:S(2)}, u32[]{:S(2)}) collective-permute-start(f32[128,256]{1,0:T(8,128)S(1)} %get-tuple-element.39), channel_id=1, source_target_pairs={{0,32},{32,64},{64,96},{1,33},{33,65},{65,97},{2,34},{34,66},{66,9... | collective-permute-start | bytes 393224 | tf_op jit(solution)/shard_map/ppermute | solution.py:303
  48.4 8.5 %collective-permute-start.7 = (f32[128,256]{1,0:T(8,128)S(1)}, f32[128,256]{1,0:T(8,128)S(1)}, u32[]{:S(2)}, u32[]{:S(2)}) collective-permute-start(f32[128,256]{1,0:T(8,128)S(1)} %get-tuple-element.39), channel_id=1, source_target_pairs={{0,64},{32,96},{1,65},{33,97},{2,66},{34,98},{3,67},{35,99},{4,68}... | collective-permute-start | bytes 393224 | tf_op jit(solution)/shard_map/ppermute | solution.py:303
  54.9 4.6 %collective-permute-start.8 = (f32[128,256]{1,0:T(8,128)S(1)}, f32[128,256]{1,0:T(8,128)S(1)}, u32[]{:S(2)}, u32[]{:S(2)}) collective-permute-start(f32[128,256]{1,0:T(8,128)S(1)} %get-tuple-element.39), channel_id=1, source_target_pairs={{0,96},{1,97},{2,98},{3,99},{4,100},{5,101},{6,102},{7,103},{8,104... | collective-permute-start | bytes 393224 | tf_op jit(solution)/shard_map/ppermute | solution.py:303
  59.5 11.6 %copy-start.6 = (bf16[512,512]{1,0:T(8,128)(2,1)S(1)}, bf16[512,512]{1,0:T(8,128)(2,1)}, u32[]{:S(2)}) copy-start(bf16[512,512]{1,0:T(8,128)(2,1)} %gate_ref.1) | copy-start | bytes 1572868
  59.5 11.6 %copy-start.8 = (f32[128]{0:T(128)S(1)}, f32[128]{0:T(128)}, u32[]{:S(2)}) copy-start(f32[128]{0:T(128)} %param.28) | copy-start | bytes 1540
  60.3 10.8 %collective-permute-start.10 = (f32[128,128]{1,0:T(8,128)S(1)}, f32[128,128]{1,0:T(8,128)S(1)}, u32[]{:S(2)}, u32[]{:S(2)}) collective-permute-start(f32[128,128]{1,0:T(8,128)S(1)} %get-tuple-element.44), channel_id=1, source_target_pairs={{0,4},{2,6},{4,0},{6,2},{1,5},{3,7},{5,1},{7,3},{8,12},{10,14},{12... | collective-permute-start | bytes 196616 | tf_op jit(solution)/shard_map/ppermute | solution.py:298
  61.4 9.8 %collective-permute-start.11 = (f32[128,128]{1,0:T(8,128)S(1)}, f32[128,128]{1,0:T(8,128)S(1)}, u32[]{:S(2)}, u32[]{:S(2)}) collective-permute-start(f32[128,128]{1,0:T(8,128)S(1)} %get-tuple-element.45), channel_id=1, source_target_pairs={{0,2},{2,4},{4,6},{6,0},{1,3},{3,5},{5,7},{7,1},{8,10},{10,12},{12... | collective-permute-start | bytes 196616 | tf_op jit(solution)/shard_map/ppermute | solution.py:298
  61.4 9.8 %collective-permute-start.9 = (f32[128,128]{1,0:T(8,128)S(1)}, f32[128,128]{1,0:T(8,128)S(1)}, u32[]{:S(2)}, u32[]{:S(2)}) collective-permute-start(f32[128,128]{1,0:T(8,128)S(1)} %get-tuple-element.43), channel_id=1, source_target_pairs={{0,6},{2,0},{4,2},{6,4},{1,7},{3,1},{5,3},{7,5},{8,14},{10,8},{12,... | collective-permute-start | bytes 196616 | tf_op jit(solution)/shard_map/ppermute | solution.py:298
  64.1 14.3 %copy-start.11 = (s32[256,4]{0,1:T(4,128)S(1)}, s32[256,4]{0,1:T(4,128)}, u32[]{:S(2)}) copy-start(s32[256,4]{0,1:T(4,128)} %param.32) | copy-start | bytes 12292
  71.1 8.4 %copy-start.7 = (f32[2048]{0:T(1024)S(1)}, f32[2048]{0:T(1024)}, u32[]{:S(2)}) copy-start(f32[2048]{0:T(1024)} %param.31) | copy-start | bytes 24580
  71.2 1.2 copy-start.4
  72.4 1.2 copy-start.5
  75.2 4.4 %collective-permute-start.12 = (bf16[256,512]{1,0:T(8,128)(2,1)S(1)}, bf16[256,512]{1,0:T(8,128)(2,1)S(1)}, u32[]{:S(2)}, u32[]{:S(2)}) collective-permute-start(bf16[256,512]{1,0:T(8,128)(2,1)S(1)} %get-tuple-element.47), channel_id=1, source_target_pairs={{0,1},{1,0},{2,3},{3,2},{4,5},{5,4},{6,7},{7,6},{8,9},{9,8},{10,11... | collective-permute-start | bytes 786440 | tf_op jit(solution)/shard_map/ppermute | solution.py:298
  78.6 8.4 %copy-start.2 = (f32[128,256]{1,0:T(8,128)}, f32[128,256]{1,0:T(8,128)S(1)}, u32[]{:S(2)}) copy-start(f32[128,256]{1,0:T(8,128)S(1)} %convolution_select_fusion.slot_ref) | copy-start | bytes 393220
  86.9 38.3 %all-to-all-start.2 = ((bf16[128,8,1024]{2,1,0:T(8,128)(2,1)}), bf16[128,8,1024]{2,1,0:T(8,128)(2,1)}, u32[]{:S(2)}, u32[]{:S(2)}) async-start(bf16[128,8,1024]{2,1,0:T(8,128)(2,1)} %get-tuple-element.49), calls=%async_computation.2 | async-start | bytes 4194304 | tf_op jit(solution)/shard_map/all_to_all | solution.py:383
  101.3 29.5 %copy-start.12 = (f32[256,4]{0,1:T(4,128)S(1)}, f32[256,4]{0,1:T(4,128)}, u32[]{:S(2)}) copy-start(f32[256,4]{0,1:T(4,128)} %param.33) | copy-start | bytes 12292
  101.3 30.5 %copy-start.3 = (f32[128,256]{1,0:T(8,128)S(1)}, f32[128,256]{1,0:T(8,128)}, u32[]{:S(2)}) copy-start(f32[128,256]{1,0:T(8,128)} %copy-done.2) | copy-start | bytes 393220
  125.3 58.2 %all-to-all-start = ((bf16[128,8,2048]{2,1,0:T(8,128)(2,1)}), bf16[128,8,2048]{2,1,0:T(8,128)(2,1)}, u32[]{:S(2)}, u32[]{:S(2)}) async-start(bf16[128,8,2048]{2,1,0:T(8,128)(2,1)} %dispatch.1), calls=%async_computation | async-start | bytes 8388608 | tf_op jit(solution)/shard_map/all_to_all | solution.py:383
  140.0 2.0 copy-start.13
  140.6 1.4 copy-start.9
  183.5 35.7 %all-to-all-start.3 = ((bf16[128,8,1024]{2,1,0:T(8,128)(2,1)}), bf16[128,8,1024]{2,1,0:T(8,128)(2,1)}, u32[]{:S(2)}, u32[]{:S(2)}) async-start(bf16[128,8,1024]{2,1,0:T(8,128)(2,1)} %reshape.233), calls=%async_computation.3 | async-start | bytes 4194304 | tf_op jit(solution)/shard_map/all_to_all | solution.py:383
  192.5 2.5 copy-start.14
  210.8 13.9 %copy-start.10 = (bf16[256,2048]{1,0:T(8,128)(2,1)S(1)}, bf16[256,2048]{1,0:T(8,128)(2,1)}, u32[]{:S(2)}) copy-start(bf16[256,2048]{1,0:T(8,128)(2,1)} %get-tuple-element.48.normed_ref) | copy-start | bytes 3145732
  219.2 58.2 %all-to-all-start.1 = ((bf16[128,8,2048]{2,1,0:T(8,128)(2,1)}), bf16[128,8,2048]{2,1,0:T(8,128)(2,1)}, u32[]{:S(2)}, u32[]{:S(2)}) async-start(bf16[128,8,2048]{2,1,0:T(8,128)(2,1)} %convert_bitcast_fusion), calls=%async_computation.1 | async-start | bytes 8388608 | tf_op jit(solution)/shard_map/all_to_all | solution.py:383
  230.6 3.6 %copy-start.15 = (bf16[256,2048]{1,0:T(8,128)(2,1)S(1)}, bf16[256,2048]{1,0:T(8,128)(2,1)}, u32[]{:S(2)}) copy-start(bf16[256,2048]{1,0:T(8,128)(2,1)} %get-tuple-element.50) | copy-start | bytes 3145732
  277.5 7.6 %copy-start.1 = (bf16[1,512,2048]{2,1,0:T(8,128)(2,1)S(1)}, bf16[1,512,2048]{2,1,0:T(8,128)(2,1)}, u32[]{:S(2)}) copy-start(bf16[1,512,2048]{2,1,0:T(8,128)(2,1)} %param.36) | copy-start | bytes 6291460
where the time goes:
time: 286 us; the launch traced here: 285 us
  waiting for transfers between devices  103 us (36%)
  Pallas kernels  56.6 us (20%)
  starting transfers between devices  53.2 us (19%)
  matrix products  39.3 us (14%)
  local copies, waits for them, and re-layouts  29.6 us (10%)
    all_to_all x4, waiting for transfers between devices, exchange(): return lax.all_to_all(rows, SP_TP, split_axis=0, concat_axis=0, tiled=True)  90.7 us
    pallas_call x2, Pallas kernels, state_maps(): pl.pallas_call(functools.partial(maps_kernel, slots), grid_spec=pltpu.Pre...  24.9 us
    all_to_all x4, starting transfers between devices, exchange(): return lax.all_to_all(rows, SP_TP, split_axis=0, concat_axis=0, tiled=True)  24.7 us
    dot_general x3, matrix products, feed_forward(): return jnp.dot(hidden, w_down, preferred_element_type=F32)  21.8 us
    ppermute x10, starting transfers between devices, ring(): lax.ppermute(array, axis, [(i, (i + step) % count) for i in range(count)])  17 us
    ppermute x3, starting transfers between devices, onward(): lax.ppermute(array, axis, [(i, i + step) for i in range(count - step)])  11.5 us
    dot_general x3, matrix products, feed_forward(): hidden = jax.nn.silu(jnp.dot(rows, w_gate, preferred_element_type=F32))  10.3 us
    ppermute x10, waiting for transfers between devices, ring(): lax.ppermute(array, axis, [(i, (i + step) % count) for i in range(count)])  9.47 us
  transfers between devices with their start and end apart: 17, of which 12 were waited for; matrix products, arithmetic and copies ran while one was open for 24% of the time, Pallas kernels for 5%

commit v1 on v0

--- a/solution.py
+++ b/solution.py
@@ -141,7 +141,8 @@
         ]
         return [inverse[r] - fine_square(parts(steps[r]), halves[r]) for r in range(number)]
 
-    inverse = lax.fori_loop(1, BLOCK.bit_length() - 1, widen, inverse)
+    for level in range(1, BLOCK.bit_length() - 1):
+        inverse = widen(level, inverse)
     highs, lows = [], []
     for r in range(number):
         here = slice(r * BLOCK, (r + 1) * BLOCK)
@@ -334,11 +335,22 @@
     return [found[0], first, two, three]
 
 
-def finish_kernel(place_ref, core_ref, qe_ref, o0_ref, gate_ref, gain_ref, *refs):
-    states, (keep_ref, send_ref, whole_ref) = refs[:-3], refs[-3:]
+def finish_kernel(place_ref, core_ref, gain_ref, *refs):
+    states, refs = refs[:-10], refs[-10:]
+    qe_hbm, o0_hbm, gate_hbm, keep_ref, send_ref, qe_ref, o0_ref, gate_ref, whole_ref, done = refs
     number = len(states)
     half = keep_ref.shape[0]
     core = core_ref[0]
+    pairs = ((qe_hbm, qe_ref), (o0_hbm, o0_ref), (gate_hbm, gate_ref))
+
+    def arrival(i, h):
+        there = pl.ds(pl.multiple_of(h * HD, HD), HD)
+        source, target = pairs[i]
+        return pltpu.make_async_copy(source.at[:, there], target.at[:, there], done.at[i, h])
+
+    for h in range(number):
+        for i in range(len(pairs)):
+            arrival(i, h).start()
 
     @pl.loop(0, number)
     def _(h):
@@ -347,6 +359,8 @@
         state = states[0][...]
         for s in range(1, number):
             state = jnp.where(slot == s, states[s][...], state)
+        for i in range(len(pairs)):
+            arrival(i, h).wait()
         mix = o0_ref[:, there] + fine(parts(qe_ref[:, there]), parts(state))
         scaled = mix * lax.rsqrt(jnp.mean(mix * mix, axis=-1, keepdims=True) + EPS)
         gate = gate_ref[:, there].astype(F32)
@@ -356,20 +370,29 @@
 
 
 def finish(qe, o0, states, gate, gain, place):
-    length, wide = qe.shape
+    length, wide = gate.shape
     small = pl.BlockSpec(memory_space=pltpu.SMEM)
-    arrays = (qe, o0, gate, gain.reshape(1, HD), *states)
+    arrays = (gain.reshape(1, HD), *states)
     return pl.pallas_call(
         finish_kernel,
-        in_specs=[small, small] + [pl.BlockSpec(memory_space=pltpu.VMEM)] * len(arrays),
+        in_specs=[small, small]
+        + [pl.BlockSpec(memory_space=pltpu.VMEM)] * len(arrays)
+        + [pl.BlockSpec(memory_space=pl.ANY)] * 3,
         out_shape=[pltpu.VMEM((length // 2, wide), BF16)] * 2,
-        scratch_shapes=[pltpu.VMEM((length, HD), F32)],
+        scratch_shapes=[
+            pltpu.VMEM((length, wide), F32),
+            pltpu.VMEM((length, wide), F32),
+            pltpu.VMEM((length, wide), BF16),
+            pltpu.VMEM((length, HD), F32),
+            pltpu.SemaphoreType.DMA((3, len(states))),
+        ],
         compiler_params=pltpu.CompilerParams(vmem_limit_bytes=12 << 20),
         name="finish",
     )(
         place,
         place_on("tp"),
         *[pltpu.with_memory_space_constraint(a, pltpu.VMEM) for a in arrays],
+        *[pltpu.with_memory_space_constraint(a, pltpu.HBM) for a in (qe, o0, gate)],
     )
 
 
@@ -422,7 +445,8 @@
 def attend_kernel(
     core_ref, keep_ref, came_ref, gain_ref, slot_ref, matrix_ref, residual_ref, *refs
 ):
-    attended_ref, normed_ref, rest_ref, wide_ref, matrix_vmem, residual_vmem, done = refs
+    attended_hbm, normed_hbm, rest_hbm, attended_ref, normed_ref, rest_ref = refs[:6]
+    wide_ref, matrix_vmem, residual_vmem, done, gone = refs[6:]
     length, dim = residual_ref.shape
     wide = keep_ref.shape[1]
     number = 4
@@ -450,10 +474,18 @@
         plain = attended.astype(F32)
         wide_ref[:, there] = plain
         squares = squares + jnp.sum(plain * plain, axis=-1, keepdims=True)
+    leaving = [pltpu.make_async_copy(attended_ref, attended_hbm, gone.at[0])]
+    leaving[0].start()
     scale = lax.rsqrt(squares / dim + EPS)
     normed_ref[...] = (wide_ref[...] * scale * gain_ref[...]).astype(BF16)
+    leaving.append(pltpu.make_async_copy(normed_ref, normed_hbm, gone.at[1]))
+    leaving[1].start()
     half = dim // 2
     count = 32
+
+    def departure(i):
+        there = pl.ds(pl.multiple_of(i * count, count), count)
+        return pltpu.make_async_copy(rest_ref.at[there], rest_hbm.at[there], gone.at[2 + i])
 
     @pl.loop(0, slot_ref.shape[0] // count)
     def _(i):
@@ -465,6 +497,12 @@
         tail = (chosen & (step >= extra)).astype(F32).astype(BF16)
         rows = dot_nn(lead, normed_ref[:, :half]) + dot_nn(tail, normed_ref[:, half:])
         rest_ref[pl.ds(start, count), :, :] = rows.astype(BF16).reshape(count, KEEP, half)
+        departure(i).start()
+
+    for i in range(slot_ref.shape[0] // count):
+        departure(i).wait()
+    for copy in leaving:
+        copy.wait()
 
 
 def attend(keep, came, out_matrix, residual, gain, slot):
@@ -477,19 +515,23 @@
         in_specs=[pl.BlockSpec(memory_space=pltpu.SMEM)]
         + [pl.BlockSpec(memory_space=pltpu.VMEM)] * len(arrays)
         + [pl.BlockSpec(memory_space=pl.ANY)] * 2,
+        out_specs=[pl.BlockSpec(memory_space=pl.ANY)] * 3,
         out_shape=[rows, rows, pltpu.HBM((experts, KEEP, dim // 2), BF16)],
         scratch_shapes=[
+            pltpu.VMEM((length, dim), BF16),
+            pltpu.VMEM((length, dim), BF16),
+            pltpu.VMEM((experts, KEEP, dim // 2), BF16),
             pltpu.VMEM((length, dim), F32),
             pltpu.VMEM(out_matrix.shape, BF16),
             pltpu.VMEM((length, dim), BF16),
             pltpu.SemaphoreType.DMA((5,)),
+            pltpu.SemaphoreType.DMA((2 + experts // 32,)),
         ],
         name="attend",
     )(
         place_on("tp"),
         *[pltpu.with_memory_space_constraint(a, pltpu.VMEM) for a in arrays],
-        out_matrix,
-        residual,
+        *[pltpu.with_memory_space_constraint(a, pltpu.HBM) for a in (out_matrix, residual)],
     )
 
 
@@ -519,26 +561,55 @@
     )(slot, normed)
 
 
-def final_kernel(table_ref, rows_ref, early_ref, out_ref):
-    out_ref[...] = (early_ref[...] + dot_nn(table_ref[...], rows_ref[...])).astype(BF16)
+def final_kernel(table_ref, early_ref, rows_ref, out_ref, early_vmem, rows_vmem, out_vmem, done):
+    number = done.shape[1]
+    block = out_vmem.shape[1] // number
+    spans = [pl.ds(c * block, block) for c in range(number)]
+    comes = [
+        pltpu.make_async_copy(rows_ref.at[:, s], rows_vmem.at[:, s], done.at[0, c])
+        for c, s in enumerate(spans)
+    ]
+    goes = [
+        pltpu.make_async_copy(out_vmem.at[:, s], out_ref.at[:, s], done.at[1, c])
+        for c, s in enumerate(spans)
+    ]
+    sums = [
+        pltpu.make_async_copy(early_ref.at[:, s], early_vmem.at[:, s], done.at[2, c])
+        for c, s in enumerate(spans)
+    ]
+    for c in range(number):
+        comes[c].start()
+        sums[c].start()
+    for c in range(number):
+        there = slice(c * block, (c + 1) * block)
+        comes[c].wait()
+        sums[c].wait()
+        total = early_vmem[:, there] + dot_nn(table_ref[...], rows_vmem[:, there])
+        out_vmem[:, there] = total.astype(BF16)
+        goes[c].start()
+    for copy in goes:
+        copy.wait()
 
 
 def final_sum(table, rows, early):
     length, wide = early.shape
-    block = wide // 8
-    column = pl.BlockSpec((length, block), lambda i: (0, i))
     return pl.pallas_call(
         final_kernel,
-        grid=(wide // block,),
-        in_specs=[
-            pl.BlockSpec(table.shape, lambda i: (0, 0)),
-            pl.BlockSpec((rows.shape[0], block), lambda i: (0, i)),
-            column,
+        in_specs=[pl.BlockSpec(memory_space=pltpu.VMEM)] + [pl.BlockSpec(memory_space=pl.ANY)] * 2,
+        out_specs=pl.BlockSpec(memory_space=pl.ANY),
+        out_shape=pltpu.HBM((length, wide), BF16),
+        scratch_shapes=[
+            pltpu.VMEM((length, wide), F32),
+            pltpu.VMEM(rows.shape, BF16),
+            pltpu.VMEM((length, wide), BF16),
+            pltpu.SemaphoreType.DMA((3, 4)),
         ],
-        out_specs=column,
-        out_shape=jax.ShapeDtypeStruct((length, wide), BF16),
+        compiler_params=pltpu.CompilerParams(vmem_limit_bytes=16 << 20),
         name="final_sum",
-    )(table, rows, early)
+    )(
+        pltpu.with_memory_space_constraint(table, pltpu.VMEM),
+        *[pltpu.with_memory_space_constraint(a, pltpu.HBM) for a in (early, rows)],
+    )
 
 
 def shards(

time: 286 us -> 272 us (0.951)
  Pallas kernels: 56.6 us -> 49 us
    pallas_call x2, Pallas kernels: 24.9 us -> 20.2 us  [state_maps(): pl.pallas_call(functools.partial(maps_kernel, slots), grid_spec=pltpu.Pre...]
    pallas_call x1, Pallas kernels: 7.62 us -> 4.3 us  [final_sum(): pl.pallas_call(final_kernel, in_specs=[pl.BlockSpec(memory_space=pltpu.VM...]
  transfers between devices with their start and end apart: 17 -> 17, of which waited for: 12 -> 10; matrix products, arithmetic and copies ran while one was open for 24% -> 25% of each run, Pallas kernels for 5% -> 9%
where the time goes in v1:
time: 272 us; the launch traced here: 271 us
  waiting for transfers between devices  102 us (38%)
  starting transfers between devices  50.6 us (19%)
  Pallas kernels  49 us (18%)
  matrix products  39.4 us (14%)
  local copies, waits for them, and re-layouts  27.5 us (10%)
    all_to_all x4, waiting for transfers between devices, exchange(): return lax.all_to_all(rows, SP_TP, split_axis=0, concat_axis=0, tiled=True)  91.1 us
    all_to_all x4, starting transfers between devices, exchange(): return lax.all_to_all(rows, SP_TP, split_axis=0, concat_axis=0, tiled=True)  22.9 us
    dot_general x3, matrix products, feed_forward(): return jnp.dot(hidden, w_down, preferred_element_type=F32)  21.8 us
    pallas_call x2, Pallas kernels, state_maps(): pl.pallas_call(functools.partial(maps_kernel, slots), grid_spec=pltpu.Pre...  20.2 us
    ppermute x10, starting transfers between devices, ring(): lax.ppermute(array, axis, [(i, (i + step) % count) for i in range(count)])  18.3 us
    dot_general x3, matrix products, feed_forward(): hidden = jax.nn.silu(jnp.dot(rows, w_gate, preferred_element_type=F32))  10.3 us
    ppermute x3, starting transfers between devices, onward(): lax.ppermute(array, axis, [(i, i + step) for i in range(count - step)])  9.45 us
    ppermute x10, waiting for transfers between devices, ring(): lax.ppermute(array, axis, [(i, (i + step) % count) for i in range(count)])  9.33 us
  transfers between devices with their start and end apart: 17, of which 10 were waited for; matrix products, arithmetic and copies ran while one was open for 25% of the time, Pallas kernels for 9%

profile of v1, /device:TPU:1, one launch (start us, length us, event | category | flops | bytes accessed | tf_op | source)
XLA Modules:
  0.0 271.1 jit_solution(1920576431356694592)
XLA Ops:
  0.0 10.2 %maps.2 = (f32[128,256]{1,0:T(8,128)S(1)}, f32[128,256]{1,0:T(8,128)S(1)}, bf16[512,1024]{1,0:T(8,128)(2,1)}, bf16[512,1024]{1,0:T(8,128)(2,1)}) custom-call(s32[1]{0:T(128)} %bitcast.12.place_ref, f32[4]{0:T(128)} %rate_ref.5, bf16[512,512]{1,0:T(8,128)(2,1)} %k_ref.5, bf16[512,512]{1,0:T(8,128)(2,1)} %v_ref.3, bf16[4,512]{1,0:T(4,128)(2,1)} %bitcast.95, ...), custom_call_target="tpu_custom_call" | custom-call | tf_op jit(solution)/shard_map/maps/pallas_call | solution.py:196
  10.2 2.0 collective-permute-start
  12.2 2.4 collective-permute-start.1
  14.6 10.0 %maps.3 = (f32[128,256]{1,0:T(8,128)S(1)}, f32[128,256]{1,0:T(8,128)S(1)}, bf16[512,1024]{1,0:T(8,128)(2,1)}, bf16[512,1024]{1,0:T(8,128)(2,1)}) custom-call(s32[1]{0:T(128)} %bitcast.12.place_ref, f32[4]{0:T(128)} %rate_ref.5, bf16[512,512]{1,0:T(8,128)(2,1)} %k_ref.5, bf16[512,512]{1,0:T(8,128)(2,1)} %v_ref.3, ...), custom_call_target="tpu_custom_call", output_to_operand_aliasing={{2}: (7, {}), {3}: (8, {})} | custom-call | tf_op jit(solution)/shard_map/maps/pallas_call | solution.py:196
  24.6 1.1 collective-permute-start.2
  25.8 0.0 collective-permute-done.1.refs_2_
  25.8 2.7 collective-permute-done.2.refs_3_
  28.5 0.6 shard_map.190
  29.1 2.8 %collective-permute-start.5 = (f32[128,256]{1,0:T(8,128)S(1)}, f32[128,256]{1,0:T(8,128)S(1)}, u32[]{:S(2)}, u32[]{:S(2)}) collective-permute-start(f32[128,256]{1,0:T(8,128)S(1)} %get-tuple-element.34.refs_0_), channel_id=1, source_target_pairs={{0,24},{8,0},{16,8},{24,16},{1,25},{9,1},{17,9},{25,17},{2,26},{10... | collective-permute-start | bytes 393224 | tf_op jit(solution)/shard_map/ppermute | solution.py:299
  31.9 0.3 collective-permute-start.4
  32.2 0.7 collective-permute-start.3
  32.9 1.9 collective-permute-done.5.refs_3_
  34.8 2.5 collective-permute-done.4.refs_2_
  37.3 1.3 collective-permute-done.3.refs_1_
  38.6 0.7 shard_map.191
  39.3 5.7 %collective-permute-start.8 = (f32[128,256]{1,0:T(8,128)S(1)}, f32[128,256]{1,0:T(8,128)S(1)}, u32[]{:S(2)}, u32[]{:S(2)}) collective-permute-start(f32[128,256]{1,0:T(8,128)S(1)} %get-tuple-element.35), channel_id=1, source_target_pairs={{0,96},{1,97},{2,98},{3,99},{4,100},{5,101},{6,102},{7,103},{8,104... | collective-permute-start | bytes 393224 | tf_op jit(solution)/shard_map/ppermute | solution.py:304
  44.9 1.3 collective-permute-start.7
  46.2 2.5 collective-permute-start.6
  48.8 1.9 collective-permute-done.6.one_ref
  50.7 0.8 shard_map.192
  51.4 2.4 collective-permute-start.9
  53.9 0.7 collective-permute-start.11
  54.5 7.0 %mixes.1 = (f32[512,512]{1,0:T(8,128)}, f32[512,512]{1,0:T(8,128)}) custom-call(f32[4]{0:T(128)} %rate_ref.5, bf16[512,512]{1,0:T(8,128)(2,1)} %q_ref.1, bf16[512,512]{1,0:T(8,128)(2,1)} %k_ref.5, bf16[4,512]{1,0:T(4,128)(2,1)} %bitcast.94, f32[4,512]{1,0:T(4,128)} %bitcast.91, bf16[512,1024]{1,0:T(8,128)(2,1)} %get-tuple-element.42.high_ref, ...), custom_call_target="tpu_custom_call" | custom-call | tf_op jit(solution)/shard_map/mixes/pallas_call | solution.py:218
  61.6 0.0 copy-start.4
  61.6 2.7 %finish.1 = (bf16[256,512]{1,0:T(8,128)(2,1)S(1)}, bf16[256,512]{1,0:T(8,128)(2,1)S(1)}) custom-call(s32[1]{0:T(128)} %bitcast.12.place_ref, s32[1]{0:T(128)} %bitcast.11.core_ref, f32[1,128]{1,0:T(1,128)S(1)} %bitcast.84, f32[128,128]{1,0:T(8,128)S(1)} %get-tuple-element.38.refs_0_, f32[128,128]{1,0:T(8,128)S(1)} %collective-permute-done.9.refs_1_, ...), custom_call_target="tpu_custom_call" | custom-call | tf_op jit(solution)/shard_map/finish/pallas_call | solution.py:376
  64.4 5.8 %collective-permute-start.12 = (bf16[256,512]{1,0:T(8,128)(2,1)S(1)}, bf16[256,512]{1,0:T(8,128)(2,1)S(1)}, u32[]{:S(2)}, u32[]{:S(2)}) collective-permute-start(bf16[256,512]{1,0:T(8,128)(2,1)S(1)} %get-tuple-element.47), channel_id=1, source_target_pairs={{0,1},{1,0},{2,3},{3,2},{4,5},{5,4},{6,7},{7,6},{8,9},{9,8},{10,11... | collective-permute-start | bytes 786440 | tf_op jit(solution)/shard_map/ppermute | solution.py:299
  70.1 0.2 convolution_select_fusion.slot_ref
  70.3 0.0 copy-start.2
  70.3 0.9 collective-permute-done.12.came_ref
  71.3 6.7 %attend.1 = (bf16[256,2048]{1,0:T(8,128)(2,1)}, bf16[256,2048]{1,0:T(8,128)(2,1)}, bf16[128,8,1024]{2,1,0:T(8,128)(2,1)}) custom-call(s32[1]{0:T(128)} %bitcast.11.core_ref, bf16[256,512]{1,0:T(8,128)(2,1)S(1)} %get-tuple-element.46.keep_ref, bf16[256,512]{1,0:T(8,128)(2,1)S(1)} %collective-permute-done.12.came_ref, f32[1,2048]{1,0:T(1,128)S(1)} %bitcast.83, ...), custom_call_target="tpu_custom_call" | custom-call | tf_op jit(solution)/shard_map/attend/pallas_call | solution.py:513
  77.9 6.4 %all-to-all-start = ((bf16[128,8,1024]{2,1,0:T(8,128)(2,1)}), bf16[128,8,1024]{2,1,0:T(8,128)(2,1)}, u32[]{:S(2)}, u32[]{:S(2)}) async-start(bf16[128,8,1024]{2,1,0:T(8,128)(2,1)} %get-tuple-element.48), calls=%async_computation | async-start | bytes 4194304 | tf_op jit(solution)/shard_map/all_to_all | solution.py:406
  84.4 6.1 %dispatch.1 = bf16[128,8,2048]{2,1,0:T(8,128)(2,1)} custom-call(f32[128,256]{1,0:T(8,128)} %copy-done.2, bf16[256,2048]{1,0:T(8,128)(2,1)} %get-tuple-element.50.normed_ref), custom_call_target="tpu_custom_call" | custom-call | tf_op jit(solution)/shard_map/dispatch/pallas_call | solution.py:551
  90.5 24.0 %all-to-all-done = bf16[128,8,1024]{2,1,0:T(8,128)(2,1)} async-done(((bf16[128,8,1024]{2,1,0:T(8,128)(2,1)}), bf16[128,8,1024]{2,1,0:T(8,128)(2,1)}, u32[]{:S(2)}, u32[]{:S(2)}) %all-to-all-start) | async-done | bytes 2097184 | tf_op jit(solution)/shard_map/all_to_all | solution.py:406
  114.5 5.5 %all-to-all-start.2 = ((bf16[128,8,2048]{2,1,0:T(8,128)(2,1)}), bf16[128,8,2048]{2,1,0:T(8,128)(2,1)}, u32[]{:S(2)}, u32[]{:S(2)}) async-start(bf16[128,8,2048]{2,1,0:T(8,128)(2,1)} %dispatch.1), calls=%async_computation.2 | async-start | bytes 8388608 | tf_op jit(solution)/shard_map/all_to_all | solution.py:406
  120.0 0.1 select_add_fusion
  120.1 0.9 broadcast_bitcast_fusion
  121.0 0.1 broadcast_bitcast_fusion.1
  121.1 4.1 %reshape.227 = bf16[128,2,4,1024]{3,2,1,0:T(4,128)(2,1)} reshape(bf16[128,8,1024]{2,1,0:T(8,128)(2,1)} %all-to-all-done) | data formatting | bytes 4194304 | tf_op jit(solution)/shard_map/reshape | solution.py:664
  125.2 4.0 %copy.36 = bf16[128,2,4,1024]{3,1,2,0:T(2,128)(2,1)S(1)} copy(bf16[128,2,4,1024]{3,2,1,0:T(4,128)(2,1)} %reshape.227) | data formatting | bytes 4194304 | tf_op jit(solution)/shard_map/reshape | solution.py:664
  129.2 0.0 copy-start.10
  129.2 0.6 copy.38
  129.8 1.4 copy-done.6
  131.2 2.2 fusion.11
  133.4 6.3 %convolution_convert_fusion = bf16[512,2048]{1,0:T(8,128)(2,1)} fusion(bf16[1,512,2048]{2,1,0:T(8,128)(2,1)S(1)} %copy-done, bf16[512,2048]{1,0:T(8,128)(2,1)} %bitcast.88, bf16[1,2048,512]{2,1,0:T(8,128)(2,1)} %param.35, f32[512,512]{1,0:T(8,128)} %fusion.11), kind=kOutput, calls=%fused_computation.5 | convolution fusion | flops 2150105088 | bytes 9437184 | tf_op jit(solution)/shard_map/dot_general | solution.py:402
  139.7 4.5 %reshape.229 = bf16[128,4,2,1024]{3,2,1,0:T(2,128)(2,1)} reshape(bf16[512,2048]{1,0:T(8,128)(2,1)} %convolution_convert_fusion) | data formatting | bytes 4194304 | tf_op jit(solution)/shard_map/reshape | solution.py:666
  144.1 4.1 %copy.37 = bf16[128,2,4,1024]{3,2,1,0:T(4,128)(2,1)} copy(bf16[128,2,4,1024]{3,1,2,0:T(2,128)(2,1)} %bitcast.86) | data formatting | bytes 4194304 | tf_op jit(solution)/shard_map/transpose | solution.py:666
  148.3 4.0 %reshape.230 = bf16[128,8,1024]{2,1,0:T(8,128)(2,1)} reshape(bf16[128,2,4,1024]{3,2,1,0:T(4,128)(2,1)} %copy.37) | data formatting | bytes 4194304 | tf_op jit(solution)/shard_map/reshape | solution.py:667
  152.2 20.5 %all-to-all-done.2 = bf16[128,8,2048]{2,1,0:T(8,128)(2,1)} async-done(((bf16[128,8,2048]{2,1,0:T(8,128)(2,1)}), bf16[128,8,2048]{2,1,0:T(8,128)(2,1)}, u32[]{:S(2)}, u32[]{:S(2)}) %all-to-all-start.2) | async-done | bytes 4194336 | tf_op jit(solution)/shard_map/all_to_all | solution.py:406
  172.7 5.5 %all-to-all-start.1 = ((bf16[128,8,1024]{2,1,0:T(8,128)(2,1)}), bf16[128,8,1024]{2,1,0:T(8,128)(2,1)}, u32[]{:S(2)}, u32[]{:S(2)}) async-start(bf16[128,8,1024]{2,1,0:T(8,128)(2,1)} %reshape.230), calls=%async_computation.1 | async-start | bytes 4194304 | tf_op jit(solution)/shard_map/all_to_all | solution.py:406
  178.2 0.1 eq.128
  178.3 2.1 copy.35
  180.4 1.3 copy.34
  181.7 1.7 fusion.30.table_ref
  183.4 0.4 copy-done.11
  183.7 5.8 %fusion.2 = f32[1024,512]{1,0:T(8,128)} fusion(bf16[128,8,2048]{2,1,0:T(8,128)(2,1)} %all-to-all-done.2, bf16[1,2048,512]{2,1,0:T(8,128)(2,1)S(1)} %copy-done.11), kind=kOutput, calls=%fused_computation.2 | convolution fusion | flops 2147483648 | bytes 8388608 | tf_op jit(solution)/shard_map/dot_general | solution.py:400
  189.5 10.1 %convert_bitcast_fusion = bf16[128,8,2048]{2,1,0:T(8,128)(2,1)} fusion(bf16[1,512,2048]{2,1,0:T(8,128)(2,1)S(1)} %copy-done, f32[1024,512]{1,0:T(8,128)} %fusion.2, bf16[1,2048,512]{2,1,0:T(8,128)(2,1)} %param.35, bf16[128,8,2048]{2,1,0:T(8,128)(2,1)} %all-to-all-done.2), kind=kOutput, calls=%fused_computation.4 | convolution fusion | flops 4300210176 | bytes 14680064 | tf_op jit(solution)/shard_map/dot_general | solution.py:402
  199.6 8.8 %all-to-all-done.1 = bf16[128,8,1024]{2,1,0:T(8,128)(2,1)} async-done(((bf16[128,8,1024]{2,1,0:T(8,128)(2,1)}), bf16[128,8,1024]{2,1,0:T(8,128)(2,1)}, u32[]{:S(2)}, u32[]{:S(2)}) %all-to-all-start.1) | async-done | bytes 2097184 | tf_op jit(solution)/shard_map/all_to_all | solution.py:406
  208.4 5.5 %all-to-all-start.3 = ((bf16[128,8,2048]{2,1,0:T(8,128)(2,1)}), bf16[128,8,2048]{2,1,0:T(8,128)(2,1)}, u32[]{:S(2)}, u32[]{:S(2)}) async-start(bf16[128,8,2048]{2,1,0:T(8,128)(2,1)} %convert_bitcast_fusion), calls=%async_computation.3 | async-start | bytes 8388608 | tf_op jit(solution)/shard_map/all_to_all | solution.py:406
  213.9 2.3 fusion.62
  216.2 3.5 %convolution_bitcast_fusion = f32[256,1024]{1,0:T(8,128)} fusion(bf16[128,8,1024]{2,1,0:T(8,128)(2,1)} %all-to-all-done.1, bf16[128,256]{1,0:T(8,128)(2,1)S(1)} %select_add_fusion, f32[128,256]{1,0:T(8,128)S(1)} %copy-done.3, f32[8]{0:T(128)S(1)} %fusion.52, pred[8]{0:T(512)(128)(4,1)S(1)} %iota_compare_fusion.6), kind=kOutput, calls=%fused_computation.17 | convolution fusion | flops 537657344 | bytes 3342376 | tf_op jit(solution)/shard_map/dot_general | solution.py:670
  219.7 3.6 %convolution_bitcast_fusion.1 = f32[256,1024]{1,0:T(8,128)} fusion(bf16[128,8,1024]{2,1,0:T(8,128)(2,1)} %all-to-all-done.1, bf16[128,256]{1,0:T(8,128)(2,1)S(1)} %select_add_fusion, f32[128,256]{1,0:T(8,128)S(1)} %copy-done.3, f32[8]{0:T(128)S(1)} %fusion.52, pred[8]{0:T(512)(128)(4,1)S(1)} %iota_compare_fusion.7), kind=kOutput, calls=%fused_computation.18 | convolution fusion | flops 537657344 | bytes 3342376 | tf_op jit(solution)/shard_map/dot_general | solution.py:670
  223.3 5.5 %fusion.4.early_ref = f32[256,2048]{1,0:T(8,128)} fusion(f32[256,1024]{1,0:T(8,128)} %convolution_bitcast_fusion, f32[256,1024]{1,0:T(8,128)} %convolution_bitcast_fusion.1, bf16[256,2048]{1,0:T(8,128)(2,1)S(1)} %copy-done.12, bf16[512,2048]{1,0:T(8,128)(2,1)} %param.39, f32[256,512]{1,0:T(8,128)S(1)} %fusion.62, bf16[256,2048]{1,0:T(8,128)(2,1)S(1)} %copy-done.7, ...), kind=kOutput, calls=%fused_computation.7 | convolution fusion | flops 1076625408 | bytes 11010048 | tf_op jit(solution)/shard_map/dot_general | solution.py:402
  228.8 37.8 %all-to-all-done.3 = bf16[128,8,2048]{2,1,0:T(8,128)(2,1)} async-done(((bf16[128,8,2048]{2,1,0:T(8,128)(2,1)}), bf16[128,8,2048]{2,1,0:T(8,128)(2,1)}, u32[]{:S(2)}, u32[]{:S(2)}) %all-to-all-start.3) | async-done | bytes 4194336 | tf_op jit(solution)/shard_map/all_to_all | solution.py:406
  266.7 4.3 %final_sum.1 = bf16[256,2048]{1,0:T(8,128)(2,1)} custom-call(bf16[256,1024]{1,0:T(8,128)(2,1)S(1)} %fusion.30.table_ref, f32[256,2048]{1,0:T(8,128)} %fusion.4.early_ref, bf16[1024,2048]{1,0:T(8,128)(2,1)} %bitcast.28.rows_ref), custom_call_target="tpu_custom_call" | custom-call | tf_op jit(solution)/shard_map/final_sum/pallas_call | solution.py:596
  (35 shorter events, 0.1 us)
Async XLA Ops:
  0.0 133.4 %copy-start = (bf16[1,512,2048]{2,1,0:T(8,128)(2,1)S(1)}, bf16[1,512,2048]{2,1,0:T(8,128)(2,1)}, u32[]{:S(2)}) copy-start(bf16[1,512,2048]{2,1,0:T(8,128)(2,1)} %param.36) | copy-start | bytes 6291460
  10.2 15.6 %collective-permute-start = (f32[128,256]{1,0:T(8,128)S(1)}, f32[128,256]{1,0:T(8,128)S(1)}, u32[]{:S(2)}, u32[]{:S(2)}) collective-permute-start(f32[128,256]{1,0:T(8,128)S(1)} %get-tuple-element.31), channel_id=1, source_target_pairs={{0,2},{2,4},{4,6},{6,0},{1,3},{3,5},{5,7},{7,1},{8,10},{10,12},{12... | collective-permute-start | bytes 393224 | tf_op jit(solution)/shard_map/ppermute | solution.py:299
  12.2 13.6 %collective-permute-start.1 = (f32[128,256]{1,0:T(8,128)S(1)}, f32[128,256]{1,0:T(8,128)S(1)}, u32[]{:S(2)}, u32[]{:S(2)}) collective-permute-start(f32[128,256]{1,0:T(8,128)S(1)} %get-tuple-element.32), channel_id=1, source_target_pairs={{0,4},{2,6},{4,0},{6,2},{1,5},{3,7},{5,1},{7,3},{8,12},{10,14},{12... | collective-permute-start | bytes 393224 | tf_op jit(solution)/shard_map/ppermute | solution.py:299
  24.6 3.8 %collective-permute-start.2 = (f32[128,256]{1,0:T(8,128)S(1)}, f32[128,256]{1,0:T(8,128)S(1)}, u32[]{:S(2)}, u32[]{:S(2)}) collective-permute-start(f32[128,256]{1,0:T(8,128)S(1)} %get-tuple-element.33), channel_id=1, source_target_pairs={{0,6},{2,0},{4,2},{6,4},{1,7},{3,1},{5,3},{7,5},{8,14},{10,8},{12,... | collective-permute-start | bytes 393224 | tf_op jit(solution)/shard_map/ppermute | solution.py:299
  29.1 5.8 %collective-permute-start.5 = (f32[128,256]{1,0:T(8,128)S(1)}, f32[128,256]{1,0:T(8,128)S(1)}, u32[]{:S(2)}, u32[]{:S(2)}) collective-permute-start(f32[128,256]{1,0:T(8,128)S(1)} %get-tuple-element.34.refs_0_), channel_id=1, source_target_pairs={{0,24},{8,0},{16,8},{24,16},{1,25},{9,1},{17,9},{25,17},{2,26},{10... | collective-permute-start | bytes 393224 | tf_op jit(solution)/shard_map/ppermute | solution.py:299
  31.9 5.4 %collective-permute-start.4 = (f32[128,256]{1,0:T(8,128)S(1)}, f32[128,256]{1,0:T(8,128)S(1)}, u32[]{:S(2)}, u32[]{:S(2)}) collective-permute-start(f32[128,256]{1,0:T(8,128)S(1)} %get-tuple-element.34.refs_0_), channel_id=1, source_target_pairs={{0,16},{8,24},{16,0},{24,8},{1,17},{9,25},{17,1},{25,9},{2,18},{10... | collective-permute-start | bytes 393224 | tf_op jit(solution)/shard_map/ppermute | solution.py:299
  32.2 6.4 %collective-permute-start.3 = (f32[128,256]{1,0:T(8,128)S(1)}, f32[128,256]{1,0:T(8,128)S(1)}, u32[]{:S(2)}, u32[]{:S(2)}) collective-permute-start(f32[128,256]{1,0:T(8,128)S(1)} %get-tuple-element.34.refs_0_), channel_id=1, source_target_pairs={{0,8},{8,16},{16,24},{24,0},{1,9},{9,17},{17,25},{25,1},{2,10},{10... | collective-permute-start | bytes 393224 | tf_op jit(solution)/shard_map/ppermute | solution.py:299
  39.3 9.5 %collective-permute-start.8 = (f32[128,256]{1,0:T(8,128)S(1)}, f32[128,256]{1,0:T(8,128)S(1)}, u32[]{:S(2)}, u32[]{:S(2)}) collective-permute-start(f32[128,256]{1,0:T(8,128)S(1)} %get-tuple-element.35), channel_id=1, source_target_pairs={{0,96},{1,97},{2,98},{3,99},{4,100},{5,101},{6,102},{7,103},{8,104... | collective-permute-start | bytes 393224 | tf_op jit(solution)/shard_map/ppermute | solution.py:304
  44.9 3.8 %collective-permute-start.7 = (f32[128,256]{1,0:T(8,128)S(1)}, f32[128,256]{1,0:T(8,128)S(1)}, u32[]{:S(2)}, u32[]{:S(2)}) collective-permute-start(f32[128,256]{1,0:T(8,128)S(1)} %get-tuple-element.35), channel_id=1, source_target_pairs={{0,64},{32,96},{1,65},{33,97},{2,66},{34,98},{3,67},{35,99},{4,68}... | collective-permute-start | bytes 393224 | tf_op jit(solution)/shard_map/ppermute | solution.py:304
  46.2 4.4 %collective-permute-start.6 = (f32[128,256]{1,0:T(8,128)S(1)}, f32[128,256]{1,0:T(8,128)S(1)}, u32[]{:S(2)}, u32[]{:S(2)}) collective-permute-start(f32[128,256]{1,0:T(8,128)S(1)} %get-tuple-element.35), channel_id=1, source_target_pairs={{0,32},{32,64},{64,96},{1,33},{33,65},{65,97},{2,34},{34,66},{66,9... | collective-permute-start | bytes 393224 | tf_op jit(solution)/shard_map/ppermute | solution.py:304
  50.7 11.0 %copy-start.5 = (f32[128]{0:T(128)S(1)}, f32[128]{0:T(128)}, u32[]{:S(2)}) copy-start(f32[128]{0:T(128)} %param.28) | copy-start | bytes 1540
  51.4 10.1 %collective-permute-start.9 = (f32[128,128]{1,0:T(8,128)S(1)}, f32[128,128]{1,0:T(8,128)S(1)}, u32[]{:S(2)}, u32[]{:S(2)}) collective-permute-start(f32[128,128]{1,0:T(8,128)S(1)} %get-tuple-element.39), channel_id=1, source_target_pairs={{0,6},{2,0},{4,2},{6,4},{1,7},{3,1},{5,3},{7,5},{8,14},{10,8},{12,... | collective-permute-start | bytes 196616 | tf_op jit(solution)/shard_map/ppermute | solution.py:299
  53.9 7.7 %collective-permute-start.10 = (f32[128,128]{1,0:T(8,128)S(1)}, f32[128,128]{1,0:T(8,128)S(1)}, u32[]{:S(2)}, u32[]{:S(2)}) collective-permute-start(f32[128,128]{1,0:T(8,128)S(1)} %get-tuple-element.40), channel_id=1, source_target_pairs={{0,4},{2,6},{4,0},{6,2},{1,5},{3,7},{5,1},{7,3},{8,12},{10,14},{12... | collective-permute-start | bytes 196616 | tf_op jit(solution)/shard_map/ppermute | solution.py:299
  53.9 7.7 %collective-permute-start.11 = (f32[128,128]{1,0:T(8,128)S(1)}, f32[128,128]{1,0:T(8,128)S(1)}, u32[]{:S(2)}, u32[]{:S(2)}) collective-permute-start(f32[128,128]{1,0:T(8,128)S(1)} %get-tuple-element.41), channel_id=1, source_target_pairs={{0,2},{2,4},{4,6},{6,0},{1,3},{3,5},{5,7},{7,1},{8,10},{10,12},{12... | collective-permute-start | bytes 196616 | tf_op jit(solution)/shard_map/ppermute | solution.py:299
  61.6 8.5 %copy-start.8 = (s32[256,4]{0,1:T(4,128)S(1)}, s32[256,4]{0,1:T(4,128)}, u32[]{:S(2)}) copy-start(s32[256,4]{0,1:T(4,128)} %param.32) | copy-start | bytes 12292
  61.6 9.7 %copy-start.4 = (f32[2048]{0:T(1024)S(1)}, f32[2048]{0:T(1024)}, u32[]{:S(2)}) copy-start(f32[2048]{0:T(1024)} %param.31) | copy-start | bytes 24580
  64.4 6.9 %collective-permute-start.12 = (bf16[256,512]{1,0:T(8,128)(2,1)S(1)}, bf16[256,512]{1,0:T(8,128)(2,1)S(1)}, u32[]{:S(2)}, u32[]{:S(2)}) collective-permute-start(bf16[256,512]{1,0:T(8,128)(2,1)S(1)} %get-tuple-element.47), channel_id=1, source_target_pairs={{0,1},{1,0},{2,3},{3,2},{4,5},{5,4},{6,7},{7,6},{8,9},{9,8},{10,11... | collective-permute-start | bytes 786440 | tf_op jit(solution)/shard_map/ppermute | solution.py:299
  70.3 7.6 %copy-start.2 = (f32[128,256]{1,0:T(8,128)}, f32[128,256]{1,0:T(8,128)S(1)}, u32[]{:S(2)}) copy-start(f32[128,256]{1,0:T(8,128)S(1)} %convolution_select_fusion.slot_ref) | copy-start | bytes 393220
  77.9 36.5 %all-to-all-start = ((bf16[128,8,1024]{2,1,0:T(8,128)(2,1)}), bf16[128,8,1024]{2,1,0:T(8,128)(2,1)}, u32[]{:S(2)}, u32[]{:S(2)}) async-start(bf16[128,8,1024]{2,1,0:T(8,128)(2,1)} %get-tuple-element.48), calls=%async_computation | async-start | bytes 4194304 | tf_op jit(solution)/shard_map/all_to_all | solution.py:406
  90.5 29.5 %copy-start.9 = (f32[256,4]{0,1:T(4,128)S(1)}, f32[256,4]{0,1:T(4,128)}, u32[]{:S(2)}) copy-start(f32[256,4]{0,1:T(4,128)} %param.33) | copy-start | bytes 12292
  90.5 30.5 %copy-start.3 = (f32[128,256]{1,0:T(8,128)S(1)}, f32[128,256]{1,0:T(8,128)}, u32[]{:S(2)}) copy-start(f32[128,256]{1,0:T(8,128)} %copy-done.2) | copy-start | bytes 393220
  114.5 58.2 %all-to-all-start.2 = ((bf16[128,8,2048]{2,1,0:T(8,128)(2,1)}), bf16[128,8,2048]{2,1,0:T(8,128)(2,1)}, u32[]{:S(2)}, u32[]{:S(2)}) async-start(bf16[128,8,2048]{2,1,0:T(8,128)(2,1)} %dispatch.1), calls=%async_computation.2 | async-start | bytes 8388608 | tf_op jit(solution)/shard_map/all_to_all | solution.py:406
  129.2 2.0 copy-start.10
  129.8 1.4 copy-start.6
  172.7 35.7 %all-to-all-start.1 = ((bf16[128,8,1024]{2,1,0:T(8,128)(2,1)}), bf16[128,8,1024]{2,1,0:T(8,128)(2,1)}, u32[]{:S(2)}, u32[]{:S(2)}) async-start(bf16[128,8,1024]{2,1,0:T(8,128)(2,1)} %reshape.230), calls=%async_computation.1 | async-start | bytes 4194304 | tf_op jit(solution)/shard_map/all_to_all | solution.py:406
  181.7 2.1 copy-start.11
  199.6 14.3 %copy-start.7 = (bf16[256,2048]{1,0:T(8,128)(2,1)S(1)}, bf16[256,2048]{1,0:T(8,128)(2,1)}, u32[]{:S(2)}) copy-start(bf16[256,2048]{1,0:T(8,128)(2,1)} %get-tuple-element.50.normed_ref) | copy-start | bytes 3145732
  208.4 58.2 %all-to-all-start.3 = ((bf16[128,8,2048]{2,1,0:T(8,128)(2,1)}), bf16[128,8,2048]{2,1,0:T(8,128)(2,1)}, u32[]{:S(2)}, u32[]{:S(2)}) async-start(bf16[128,8,2048]{2,1,0:T(8,128)(2,1)} %convert_bitcast_fusion), calls=%async_computation.3 | async-start | bytes 8388608 | tf_op jit(solution)/shard_map/all_to_all | solution.py:406
  219.7 3.6 %copy-start.12 = (bf16[256,2048]{1,0:T(8,128)(2,1)S(1)}, bf16[256,2048]{1,0:T(8,128)(2,1)}, u32[]{:S(2)}) copy-start(bf16[256,2048]{1,0:T(8,128)(2,1)} %get-tuple-element.49) | copy-start | bytes 3145732
  266.7 4.3 %copy-start.1 = (bf16[1,512,2048]{2,1,0:T(8,128)(2,1)S(1)}, bf16[1,512,2048]{2,1,0:T(8,128)(2,1)}, u32[]{:S(2)}) copy-start(bf16[1,512,2048]{2,1,0:T(8,128)(2,1)} %param.36) | copy-start | bytes 6291460

commit v2 on v1

--- a/solution.py
+++ b/solution.py
@@ -1,5 +1,3 @@
-import functools
-
 import jax
 import jax.numpy as jnp
 from jax import lax
@@ -78,8 +76,8 @@
     return g_row, jnp.broadcast_to(g_row, (HD, length)).T
 
 
-def unit(ref):
-    x = ref[...].astype(F32)
+def unit(raw):
+    x = raw.astype(F32)
     active = x * jax.nn.sigmoid(x)
     return active * lax.rsqrt(jnp.sum(active * active, axis=-1, keepdims=True) + EPS)
 
@@ -105,72 +103,75 @@
     return blocks
 
 
-def head_at(slots, step, place, heads):
-    return (place + jnp.where(step == 0, slots[0], slots[1])) % heads
-
-
-def maps_kernel(slots, place_ref, rate_ref, k_ref, v_ref, write_ref, decay_ref, extra_ref, *refs):
-    one_ref, two_ref, high_ref, low_ref = refs[-4:]
+PAIR = 2
+
+
+def maps_kernel(place_ref, rate_ref, k_ref, v_ref, write_ref, decay_ref, extra_ref, *refs):
+    map_refs, (high_ref, low_ref) = refs[:-2], refs[-2:]
+    heads = len(map_refs)
     length = k_ref.shape[0]
     number = length // BLOCK
-    step = pl.program_id(0)
-    head = head_at(slots, step, place_ref[0], rate_ref.shape[0])
-    g_row, g_col = decay_sums(rate_ref, decay_ref, extra_ref, head)
-    beta = jax.nn.sigmoid(own_row(write_ref, head))
-    b_col = jnp.broadcast_to(beta, (HD, length)).T
-    keys = unit(k_ref)
-    raw = v_ref[...].astype(F32)
-    values = raw * jax.nn.sigmoid(raw)
-    k_beta = keys * b_col
-    right = cols_of(k_beta * jnp.exp(g_col), values * b_col)
-    g_last = g_col[length - 1 : length, :]
-    k_late = parts(keys * jnp.exp(g_last - g_col))
-    lower = against_keys(parts(k_beta), parts(keys), number, g_row, g_col)
     ii = lax.broadcasted_iota(jnp.int32, (BLOCK, BLOCK), 0)
     jj = lax.broadcasted_iota(jnp.int32, (BLOCK, BLOCK), 1)
     eye = (ii == jj).astype(F32)
+    pair = range(PAIR)
+    heads_here = [pl.program_id(0) * PAIR + p for p in pair]
+    lower, right, late, last = [], [], [], []
+    for p in pair:
+        there = slice(p * HD, (p + 1) * HD)
+        g_row, g_col = decay_sums(rate_ref, decay_ref, extra_ref, heads_here[p])
+        beta = jax.nn.sigmoid(own_row(write_ref, heads_here[p]))
+        b_col = jnp.broadcast_to(beta, (HD, length)).T
+        keys = unit(k_ref[:, there])
+        raw = v_ref[:, there].astype(F32)
+        values = raw * jax.nn.sigmoid(raw)
+        k_beta = keys * b_col
+        right.append(cols_of(k_beta * jnp.exp(g_col), values * b_col))
+        last.append(g_col[length - 1 : length, :])
+        late.append(parts(keys * jnp.exp(last[p] - g_col)))
+        lower.append(against_keys(parts(k_beta), parts(keys), number, g_row, g_col))
     near = (ii // 2 == jj // 2) & (ii > jj)
-    inverse = [eye - jnp.where(near, lower[r][r], 0.0) for r in range(number)]
-
-    def widen(level, inverse):
+    chains = [(p, r) for r in range(number) for p in pair]
+    inverse = {(p, r): eye - jnp.where(near, lower[p][r][r], 0.0) for p, r in chains}
+    for level in range(1, BLOCK.bit_length() - 1):
         chosen = (ii >> (level + 1) == jj >> (level + 1)) & (ii >> level > jj >> level)
-        halves = [parts(t) for t in inverse]
-        steps = [
-            fine_square(halves[r], parts(jnp.where(chosen, lower[r][r], 0.0)))
-            for r in range(number)
-        ]
-        return [inverse[r] - fine_square(parts(steps[r]), halves[r]) for r in range(number)]
-
-    for level in range(1, BLOCK.bit_length() - 1):
-        inverse = widen(level, inverse)
-    highs, lows = [], []
-    for r in range(number):
+        halves = {c: parts(inverse[c]) for c in chains}
+        steps = {
+            (p, r): fine_square(halves[p, r], parts(jnp.where(chosen, lower[p][r][r], 0.0)))
+            for p, r in chains
+        }
+        inverse = {c: inverse[c] - fine_square(parts(steps[c]), halves[c]) for c in chains}
+    highs, lows = [[] for _ in pair], [[] for _ in pair]
+    for p, r in chains:
         here = slice(r * BLOCK, (r + 1) * BLOCK)
-        rest = right[here]
+        there = slice(2 * p * HD, 2 * (p + 1) * HD)
+        rest = right[p][here]
         if r > 0:
-            known = (rows_of(*highs), rows_of(*lows))
-            rest = rest - fine(parts(cols_of(*lower[r][:r])), known)
-        one = parts(fine(parts(inverse[r]), parts(rest)))
-        highs.append(one[0])
-        lows.append(one[1])
-        high_ref[here, :] = one[0]
-        low_ref[here, :] = one[1]
-    high, low = rows_of(*highs), rows_of(*lows)
-    moved = dot_tn(rows_of(*k_late), rows_of(high, high)) + dot_tn(k_late[0], low)
-    whole = cols_of(eye * jnp.exp(g_last) - moved[:, :HD], moved[:, HD:])
-    for k, map_ref in enumerate((one_ref, two_ref)):
-
-        @pl.when(step == k)
-        def _(map_ref=map_ref):
-            map_ref[...] = whole
+            known = (rows_of(*highs[p]), rows_of(*lows[p]))
+            rest = rest - fine(parts(cols_of(*lower[p][r][:r])), known)
+        one = parts(fine(parts(inverse[p, r]), parts(rest)))
+        highs[p].append(one[0])
+        lows[p].append(one[1])
+        high_ref[here, there] = one[0]
+        low_ref[here, there] = one[1]
+    for p in pair:
+        high, low = rows_of(*highs[p]), rows_of(*lows[p])
+        moved = dot_tn(rows_of(*late[p]), rows_of(high, high)) + dot_tn(late[p][0], low)
+        whole = cols_of(eye * jnp.exp(last[p]) - moved[:, :HD], moved[:, HD:])
+        slot = (heads_here[p] + heads - place_ref[0]) % heads
+        for s, map_ref in enumerate(map_refs):
+
+            @pl.when(slot == s)
+            def _(map_ref=map_ref, whole=whole):
+                map_ref[...] = whole
 
 
 def mixes_kernel(rate_ref, q_ref, k_ref, decay_ref, extra_ref, high_ref, low_ref, qe_ref, o0_ref):
     length = q_ref.shape[0]
     number = length // BLOCK
     g_row, g_col = decay_sums(rate_ref, decay_ref, extra_ref, pl.program_id(0))
-    queries = unit(q_ref)
-    mixing = against_keys(parts(queries), parts(unit(k_ref)), number, g_row, g_col)
+    queries = unit(q_ref[...])
+    mixing = against_keys(parts(queries), parts(unit(k_ref[...])), number, g_row, g_col)
     grown = queries * jnp.exp(g_col)
     for r in range(number):
         here = slice(r * BLOCK, (r + 1) * BLOCK)
@@ -180,32 +181,24 @@
         o0_ref[here, :] = mixed[:, HD:]
 
 
-def state_maps(slots, keys, values, write_logits, decays, rates, place, filled):
+def state_maps(keys, values, write_logits, decays, rates, place):
     length, wide = keys.shape
     heads = wide // HD
-
-    def whose(step, place_ref):
-        return 0, head_at(slots, step, place_ref[0], heads)
-
-    column = pl.BlockSpec((length, HD), whose)
-    double = pl.BlockSpec((length, 2 * HD), whose)
-    table = pl.BlockSpec((heads, length), lambda step, place_ref: (0, 0))
+    column = pl.BlockSpec((length, PAIR * HD), lambda step: (0, step))
+    double = pl.BlockSpec((length, 2 * PAIR * HD), lambda step: (0, step))
+    table = pl.BlockSpec((heads, length), lambda step: (0, 0))
     small = pl.BlockSpec(memory_space=pltpu.SMEM)
-    one_map = pl.BlockSpec((HD, 2 * HD), lambda step, place_ref: (0, 0))
-    kept = [pl.BlockSpec(memory_space=pl.ANY)] * len(filled)
-    return pl.pallas_call(
-        functools.partial(maps_kernel, slots),
-        grid_spec=pltpu.PrefetchScalarGridSpec(
-            num_scalar_prefetch=1,
-            grid=(2,),
-            in_specs=[small, column, column, table, table, table] + kept,
-            out_specs=[one_map, one_map, double, double],
-        ),
-        out_shape=[pltpu.VMEM((HD, 2 * HD), F32)] * 2
+    one_map = pl.BlockSpec((HD, 2 * HD), lambda step: (0, 0))
+    out = pl.pallas_call(
+        maps_kernel,
+        grid=(heads // PAIR,),
+        in_specs=[small, small, column, column, table, table, table],
+        out_specs=[one_map] * heads + [double, double],
+        out_shape=[pltpu.VMEM((HD, 2 * HD), F32)] * heads
         + [jax.ShapeDtypeStruct((length, 2 * wide), BF16)] * 2,
-        input_output_aliases={7: 2, 8: 3} if filled else {},
         name="maps",
-    )(place, rates, keys, values, write_logits.T, *decays, *filled)
+    )(place, rates, keys, values, write_logits.T, *decays)
+    return out[:heads], out[heads], out[heads + 1]
 
 
 def mixes(queries, keys, decays, rates, high, low):
@@ -314,8 +307,7 @@
     many = pltpu.VMEM((number,) + own.shape, F32)
     held = [pltpu.VMEM((number,) + own.shape, F32)]
     inner, line = small_call(all_before_kernel, [many, one], held, place, own, *arrived)
-    two = ring(line, "sp_1", 2)
-    first, three = [ring(line, "sp_1", s) for s in (1, 3)]
+    two, first, three = [ring(line, "sp_1", s) for s in (2, 1, 3)]
     middle, plane = small_call(
         mine_before_kernel, [one, one], held, place_on("sp_1"), line, first, two, three
     )
@@ -636,12 +628,17 @@
 ):
     place = place_on("sp_2")
     decays = (decay_input_logits.T, extra_log_decay.T)
-    base = (projected_keys, projected_values, write_strength_logits, decays, head_rate_logarithm)
-    far, near, high, low = state_maps((2, 1), *base, place, ())
+    (own, near, far, last), high, low = state_maps(
+        projected_keys,
+        projected_values,
+        write_strength_logits,
+        decays,
+        head_rate_logarithm,
+        place,
+    )
     far = ring(far, "sp_2", 2)
-    near = ring(near, "sp_2", 1)
-    last, own, high, low = state_maps((3, 0), *base, place, (high, low))
-    states = entering(own, (near, far, ring(last, "sp_2", 3)), place)
+    near, last = ring(near, "sp_2", 1), ring(last, "sp_2", 3)
+    states = entering(own, (near, far, last), place)
     qe, o0 = mixes(projected_queries, projected_keys, decays, head_rate_logarithm, high, low)
     keep, send = finish(qe, o0, states, output_gate_values, per_head_norm_gain, place)
     came = ring(send, "tp", 1)

time: 272 us -> 270 us (level)
  Pallas kernels: 49 us -> 42.9 us
  waiting for transfers between devices: 102 us -> 107 us
    pallas_call x2 -> x1, Pallas kernels: 20.2 us -> 13.9 us  [state_maps(): pl.pallas_call(maps_kernel, grid=(heads // PAIR,), in_specs=[small, small...]
    ppermute x10, waiting for transfers between devices: 9.33 us -> 13.3 us  [ring(): lax.ppermute(array, axis, [(i, (i + step) % count) for i in range(count)])]
    ppermute x10, starting transfers between devices: 18.3 us -> 15.4 us  [ring(): lax.ppermute(array, axis, [(i, (i + step) % count) for i in range(count)])]
  transfers between devices with their start and end apart: 17 -> 17, of which waited for: 10 -> 11; matrix products, arithmetic and copies ran while one was open for 25% -> 25% of each run, Pallas kernels for 9% -> 5%
where the time goes in v2:
time: 270 us; the launch traced here: 268 us
  waiting for transfers between devices  107 us (40%)
  starting transfers between devices  49.4 us (18%)
  Pallas kernels  42.9 us (16%)
  matrix products  39.4 us (15%)
  local copies, waits for them, and re-layouts  27.6 us (10%)
    all_to_all x4, waiting for transfers between devices, exchange(): return lax.all_to_all(rows, SP_TP, split_axis=0, concat_axis=0, tiled=True)  90.9 us
    all_to_all x4, starting transfers between devices, exchange(): return lax.all_to_all(rows, SP_TP, split_axis=0, concat_axis=0, tiled=True)  24.6 us
    dot_general x3, matrix products, feed_forward(): return jnp.dot(hidden, w_down, preferred_element_type=F32)  21.8 us
    ppermute x10, starting transfers between devices, ring(): lax.ppermute(array, axis, [(i, (i + step) % count) for i in range(count)])  15.4 us
    pallas_call x1, Pallas kernels, state_maps(): pl.pallas_call(maps_kernel, grid=(heads // PAIR,), in_specs=[small, small...  13.9 us
    ppermute x10, waiting for transfers between devices, ring(): lax.ppermute(array, axis, [(i, (i + step) % count) for i in range(count)])  13.3 us
    dot_general x3, matrix products, feed_forward(): hidden = jax.nn.silu(jnp.dot(rows, w_gate, preferred_element_type=F32))  10.3 us
    ppermute x3, starting transfers between devices, onward(): lax.ppermute(array, axis, [(i, i + step) for i in range(count - step)])  9.44 us
  transfers between devices with their start and end apart: 17, of which 11 were waited for; matrix products, arithmetic and copies ran while one was open for 25% of the time, Pallas kernels for 5%

profile of v2, /device:TPU:1, one launch (start us, length us, event | category | flops | bytes accessed | tf_op | source)
XLA Modules:
  0.0 268.5 jit_solution(4067645597915205445)
XLA Ops:
  0.0 13.9 %maps.1 = (f32[128,256]{1,0:T(8,128)S(1)}, f32[128,256]{1,0:T(8,128)S(1)}, f32[128,256]{1,0:T(8,128)S(1)}, f32[128,256]{1,0:T(8,128)S(1)}, bf16[512,1024]{1,0:T(8,128)(2,1)}, /*index=5*/bf16[512,1024]{1,0:T(8,128)(2,1)}) custom-call(s32[1]{0:T(128)} %bitcast.12.place_ref, f32[4]{0:T(128)} %rate_ref.3, bf16[512,512]{1,0:T(8,128)(2,1)} %k_ref.3, ...), custom_call_target="tpu_custom_call" | custom-call | tf_op jit(solution)/shard_map/maps/pallas_call | solution.py:192
  13.9 2.0 collective-permute-start
  16.0 2.4 collective-permute-start.1
  18.4 1.2 collective-permute-start.2
  19.6 0.5 collective-permute-done.refs_1_
  20.1 4.1 %collective-permute-done.1.refs_2_ = f32[128,256]{1,0:T(8,128)S(1)} collective-permute-done((f32[128,256]{1,0:T(8,128)S(1)}, f32[128,256]{1,0:T(8,128)S(1)}, u32[]{:S(2)}, u32[]{:S(2)}) %collective-permute-start.1) | collective-permute-done | bytes 131104 | tf_op jit(solution)/shard_map/ppermute | solution.py:292
  24.1 0.6 shard_map.190
  24.8 2.8 %collective-permute-start.5 = (f32[128,256]{1,0:T(8,128)S(1)}, f32[128,256]{1,0:T(8,128)S(1)}, u32[]{:S(2)}, u32[]{:S(2)}) collective-permute-start(f32[128,256]{1,0:T(8,128)S(1)} %get-tuple-element.30.refs_0_), channel_id=1, source_target_pairs={{0,24},{8,0},{16,8},{24,16},{1,25},{9,1},{17,9},{25,17},{2,26},{10... | collective-permute-start | bytes 393224 | tf_op jit(solution)/shard_map/ppermute | solution.py:292
  27.6 0.3 collective-permute-start.4
  27.9 0.7 collective-permute-start.3
  28.6 1.4 collective-permute-done.5.refs_3_
  30.0 3.0 %collective-permute-done.4.refs_2_ = f32[128,256]{1,0:T(8,128)S(1)} collective-permute-done((f32[128,256]{1,0:T(8,128)S(1)}, f32[128,256]{1,0:T(8,128)S(1)}, u32[]{:S(2)}, u32[]{:S(2)}) %collective-permute-start.4) | collective-permute-done | bytes 131104 | tf_op jit(solution)/shard_map/ppermute | solution.py:292
  33.0 3.4 %collective-permute-done.3.refs_1_ = f32[128,256]{1,0:T(8,128)S(1)} collective-permute-done((f32[128,256]{1,0:T(8,128)S(1)}, f32[128,256]{1,0:T(8,128)S(1)}, u32[]{:S(2)}, u32[]{:S(2)}) %collective-permute-start.3) | collective-permute-done | bytes 131104 | tf_op jit(solution)/shard_map/ppermute | solution.py:292
  36.4 0.7 shard_map.191
  37.0 5.7 %collective-permute-start.8 = (f32[128,256]{1,0:T(8,128)S(1)}, f32[128,256]{1,0:T(8,128)S(1)}, u32[]{:S(2)}, u32[]{:S(2)}) collective-permute-start(f32[128,256]{1,0:T(8,128)S(1)} %get-tuple-element.31), channel_id=1, source_target_pairs={{0,96},{1,97},{2,98},{3,99},{4,100},{5,101},{6,102},{7,103},{8,104... | collective-permute-start | bytes 393224 | tf_op jit(solution)/shard_map/ppermute | solution.py:297
  42.7 1.3 collective-permute-start.7
  44.0 2.5 collective-permute-start.6
  46.5 0.0 collective-permute-done.7.two_ref
  46.5 2.7 collective-permute-done.6.one_ref
  49.2 0.8 shard_map.192
  50.0 2.4 collective-permute-start.9
  52.3 0.9 collective-permute-start.10
  53.2 7.1 %mixes.1 = (f32[512,512]{1,0:T(8,128)}, f32[512,512]{1,0:T(8,128)}) custom-call(f32[4]{0:T(128)} %rate_ref.3, bf16[512,512]{1,0:T(8,128)(2,1)} %q_ref.1, bf16[512,512]{1,0:T(8,128)(2,1)} %k_ref.3, bf16[4,512]{1,0:T(4,128)(2,1)} %bitcast.92, f32[4,512]{1,0:T(4,128)} %bitcast.90, bf16[512,1024]{1,0:T(8,128)(2,1)} %get-tuple-element.38.high_ref, ...), custom_call_target="tpu_custom_call" | custom-call | tf_op jit(solution)/shard_map/mixes/pallas_call | solution.py:211
  60.3 0.0 copy-start.4
  60.3 2.7 %finish.1 = (bf16[256,512]{1,0:T(8,128)(2,1)S(1)}, bf16[256,512]{1,0:T(8,128)(2,1)S(1)}) custom-call(s32[1]{0:T(128)} %bitcast.12.place_ref, s32[1]{0:T(128)} %bitcast.11.core_ref, f32[1,128]{1,0:T(1,128)S(1)} %bitcast.84, f32[128,128]{1,0:T(8,128)S(1)} %get-tuple-element.34.refs_0_, f32[128,128]{1,0:T(8,128)S(1)} %collective-permute-done.9.refs_1_, ...), custom_call_target="tpu_custom_call" | custom-call | tf_op jit(solution)/shard_map/finish/pallas_call | solution.py:368
  63.0 2.7 %collective-permute-start.12 = (bf16[256,512]{1,0:T(8,128)(2,1)S(1)}, bf16[256,512]{1,0:T(8,128)(2,1)S(1)}, u32[]{:S(2)}, u32[]{:S(2)}) collective-permute-start(bf16[256,512]{1,0:T(8,128)(2,1)S(1)} %get-tuple-element.43), channel_id=1, source_target_pairs={{0,1},{1,0},{2,3},{3,2},{4,5},{5,4},{6,7},{7,6},{8,9},{9,8},{10,11... | collective-permute-start | bytes 786440 | tf_op jit(solution)/shard_map/ppermute | solution.py:292
  65.8 0.2 convolution_select_fusion.slot_ref
  66.0 0.0 copy-start.2
  66.0 0.9 collective-permute-done.12.came_ref
  66.9 6.7 %attend.1 = (bf16[256,2048]{1,0:T(8,128)(2,1)}, bf16[256,2048]{1,0:T(8,128)(2,1)}, bf16[128,8,1024]{2,1,0:T(8,128)(2,1)}) custom-call(s32[1]{0:T(128)} %bitcast.11.core_ref, bf16[256,512]{1,0:T(8,128)(2,1)S(1)} %get-tuple-element.42.keep_ref, bf16[256,512]{1,0:T(8,128)(2,1)S(1)} %collective-permute-done.12.came_ref, f32[1,2048]{1,0:T(1,128)S(1)} %bitcast.83, ...), custom_call_target="tpu_custom_call" | custom-call | tf_op jit(solution)/shard_map/attend/pallas_call | solution.py:505
  73.6 8.1 %all-to-all-start = ((bf16[128,8,1024]{2,1,0:T(8,128)(2,1)}), bf16[128,8,1024]{2,1,0:T(8,128)(2,1)}, u32[]{:S(2)}, u32[]{:S(2)}) async-start(bf16[128,8,1024]{2,1,0:T(8,128)(2,1)} %get-tuple-element.44), calls=%async_computation | async-start | bytes 4194304 | tf_op jit(solution)/shard_map/all_to_all | solution.py:398
  81.7 6.2 %dispatch.1 = bf16[128,8,2048]{2,1,0:T(8,128)(2,1)} custom-call(f32[128,256]{1,0:T(8,128)} %copy-done.2, bf16[256,2048]{1,0:T(8,128)(2,1)} %get-tuple-element.46.normed_ref), custom_call_target="tpu_custom_call" | custom-call | tf_op jit(solution)/shard_map/dispatch/pallas_call | solution.py:543
  87.9 23.9 %all-to-all-done = bf16[128,8,1024]{2,1,0:T(8,128)(2,1)} async-done(((bf16[128,8,1024]{2,1,0:T(8,128)(2,1)}), bf16[128,8,1024]{2,1,0:T(8,128)(2,1)}, u32[]{:S(2)}, u32[]{:S(2)}) %all-to-all-start) | async-done | bytes 2097184 | tf_op jit(solution)/shard_map/all_to_all | solution.py:398
  111.8 5.5 %all-to-all-start.2 = ((bf16[128,8,2048]{2,1,0:T(8,128)(2,1)}), bf16[128,8,2048]{2,1,0:T(8,128)(2,1)}, u32[]{:S(2)}, u32[]{:S(2)}) async-start(bf16[128,8,2048]{2,1,0:T(8,128)(2,1)} %dispatch.1), calls=%async_computation.2 | async-start | bytes 8388608 | tf_op jit(solution)/shard_map/all_to_all | solution.py:398
  117.4 0.1 select_add_fusion
  117.4 0.9 broadcast_bitcast_fusion
  118.3 0.1 broadcast_bitcast_fusion.1
  118.4 4.1 %reshape.227 = bf16[128,2,4,1024]{3,2,1,0:T(4,128)(2,1)} reshape(bf16[128,8,1024]{2,1,0:T(8,128)(2,1)} %all-to-all-done) | data formatting | bytes 4194304 | tf_op jit(solution)/shard_map/reshape | solution.py:661
  122.5 4.0 %copy.34 = bf16[128,2,4,1024]{3,1,2,0:T(2,128)(2,1)S(1)} copy(bf16[128,2,4,1024]{3,2,1,0:T(4,128)(2,1)} %reshape.227) | data formatting | bytes 4194304 | tf_op jit(solution)/shard_map/reshape | solution.py:661
  126.5 0.0 copy-start.10
  126.5 0.6 copy.36
  127.2 1.4 copy-done.6
  128.5 2.2 fusion.11
  130.8 6.3 %convolution_convert_fusion = bf16[512,2048]{1,0:T(8,128)(2,1)} fusion(bf16[1,512,2048]{2,1,0:T(8,128)(2,1)S(1)} %copy-done, bf16[512,2048]{1,0:T(8,128)(2,1)} %bitcast.88, bf16[1,2048,512]{2,1,0:T(8,128)(2,1)} %param.35, f32[512,512]{1,0:T(8,128)} %fusion.11), kind=kOutput, calls=%fused_computation.5 | convolution fusion | flops 2150105088 | bytes 9437184 | tf_op jit(solution)/shard_map/dot_general | solution.py:394
  137.0 4.5 %reshape.229 = bf16[128,4,2,1024]{3,2,1,0:T(2,128)(2,1)} reshape(bf16[512,2048]{1,0:T(8,128)(2,1)} %convolution_convert_fusion) | data formatting | bytes 4194304 | tf_op jit(solution)/shard_map/reshape | solution.py:663
  141.5 4.1 %copy.35 = bf16[128,2,4,1024]{3,2,1,0:T(4,128)(2,1)} copy(bf16[128,2,4,1024]{3,1,2,0:T(2,128)(2,1)} %bitcast.86) | data formatting | bytes 4194304 | tf_op jit(solution)/shard_map/transpose | solution.py:663
  145.7 4.0 %reshape.230 = bf16[128,8,1024]{2,1,0:T(8,128)(2,1)} reshape(bf16[128,2,4,1024]{3,2,1,0:T(4,128)(2,1)} %copy.35) | data formatting | bytes 4194304 | tf_op jit(solution)/shard_map/reshape | solution.py:664
  149.6 20.4 %all-to-all-done.2 = bf16[128,8,2048]{2,1,0:T(8,128)(2,1)} async-done(((bf16[128,8,2048]{2,1,0:T(8,128)(2,1)}), bf16[128,8,2048]{2,1,0:T(8,128)(2,1)}, u32[]{:S(2)}, u32[]{:S(2)}) %all-to-all-start.2) | async-done | bytes 4194336 | tf_op jit(solution)/shard_map/all_to_all | solution.py:398
  170.0 5.5 %all-to-all-start.1 = ((bf16[128,8,1024]{2,1,0:T(8,128)(2,1)}), bf16[128,8,1024]{2,1,0:T(8,128)(2,1)}, u32[]{:S(2)}, u32[]{:S(2)}) async-start(bf16[128,8,1024]{2,1,0:T(8,128)(2,1)} %reshape.230), calls=%async_computation.1 | async-start | bytes 4194304 | tf_op jit(solution)/shard_map/all_to_all | solution.py:398
  175.5 0.1 eq.128
  175.6 2.1 copy.33
  177.7 1.3 copy.32
  179.0 1.7 fusion.30.table_ref
  180.7 0.4 copy-done.11
  181.1 5.8 %fusion.2 = f32[1024,512]{1,0:T(8,128)} fusion(bf16[128,8,2048]{2,1,0:T(8,128)(2,1)} %all-to-all-done.2, bf16[1,2048,512]{2,1,0:T(8,128)(2,1)S(1)} %copy-done.11), kind=kOutput, calls=%fused_computation.2 | convolution fusion | flops 2147483648 | bytes 8388608 | tf_op jit(solution)/shard_map/dot_general | solution.py:392
  186.9 10.1 %convert_bitcast_fusion = bf16[128,8,2048]{2,1,0:T(8,128)(2,1)} fusion(bf16[1,512,2048]{2,1,0:T(8,128)(2,1)S(1)} %copy-done, f32[1024,512]{1,0:T(8,128)} %fusion.2, bf16[1,2048,512]{2,1,0:T(8,128)(2,1)} %param.35, bf16[128,8,2048]{2,1,0:T(8,128)(2,1)} %all-to-all-done.2), kind=kOutput, calls=%fused_computation.4 | convolution fusion | flops 4300210176 | bytes 14680064 | tf_op jit(solution)/shard_map/dot_general | solution.py:394
  197.0 8.8 %all-to-all-done.1 = bf16[128,8,1024]{2,1,0:T(8,128)(2,1)} async-done(((bf16[128,8,1024]{2,1,0:T(8,128)(2,1)}), bf16[128,8,1024]{2,1,0:T(8,128)(2,1)}, u32[]{:S(2)}, u32[]{:S(2)}) %all-to-all-start.1) | async-done | bytes 2097184 | tf_op jit(solution)/shard_map/all_to_all | solution.py:398
  205.8 5.5 %all-to-all-start.3 = ((bf16[128,8,2048]{2,1,0:T(8,128)(2,1)}), bf16[128,8,2048]{2,1,0:T(8,128)(2,1)}, u32[]{:S(2)}, u32[]{:S(2)}) async-start(bf16[128,8,2048]{2,1,0:T(8,128)(2,1)} %convert_bitcast_fusion), calls=%async_computation.3 | async-start | bytes 8388608 | tf_op jit(solution)/shard_map/all_to_all | solution.py:398
  211.3 2.3 fusion.62
  213.6 3.5 %convolution_bitcast_fusion = f32[256,1024]{1,0:T(8,128)} fusion(bf16[128,8,1024]{2,1,0:T(8,128)(2,1)} %all-to-all-done.1, bf16[128,256]{1,0:T(8,128)(2,1)S(1)} %select_add_fusion, f32[128,256]{1,0:T(8,128)S(1)} %copy-done.3, f32[8]{0:T(128)S(1)} %fusion.52, pred[8]{0:T(512)(128)(4,1)S(1)} %iota_compare_fusion.6), kind=kOutput, calls=%fused_computation.17 | convolution fusion | flops 537657344 | bytes 3342376 | tf_op jit(solution)/shard_map/dot_general | solution.py:667
  217.1 3.6 %convolution_bitcast_fusion.1 = f32[256,1024]{1,0:T(8,128)} fusion(bf16[128,8,1024]{2,1,0:T(8,128)(2,1)} %all-to-all-done.1, bf16[128,256]{1,0:T(8,128)(2,1)S(1)} %select_add_fusion, f32[128,256]{1,0:T(8,128)S(1)} %copy-done.3, f32[8]{0:T(128)S(1)} %fusion.52, pred[8]{0:T(512)(128)(4,1)S(1)} %iota_compare_fusion.7), kind=kOutput, calls=%fused_computation.18 | convolution fusion | flops 537657344 | bytes 3342376 | tf_op jit(solution)/shard_map/dot_general | solution.py:667
  220.7 5.5 %fusion.4.early_ref = f32[256,2048]{1,0:T(8,128)} fusion(f32[256,1024]{1,0:T(8,128)} %convolution_bitcast_fusion, f32[256,1024]{1,0:T(8,128)} %convolution_bitcast_fusion.1, bf16[256,2048]{1,0:T(8,128)(2,1)S(1)} %copy-done.12, bf16[512,2048]{1,0:T(8,128)(2,1)} %param.39, f32[256,512]{1,0:T(8,128)S(1)} %fusion.62, bf16[256,2048]{1,0:T(8,128)(2,1)S(1)} %copy-done.7, ...), kind=kOutput, calls=%fused_computation.7 | convolution fusion | flops 1076625408 | bytes 11010048 | tf_op jit(solution)/shard_map/dot_general | solution.py:394
  226.2 37.8 %all-to-all-done.3 = bf16[128,8,2048]{2,1,0:T(8,128)(2,1)} async-done(((bf16[128,8,2048]{2,1,0:T(8,128)(2,1)}), bf16[128,8,2048]{2,1,0:T(8,128)(2,1)}, u32[]{:S(2)}, u32[]{:S(2)}) %all-to-all-start.3) | async-done | bytes 4194336 | tf_op jit(solution)/shard_map/all_to_all | solution.py:398
  264.0 4.3 %final_sum.1 = bf16[256,2048]{1,0:T(8,128)(2,1)} custom-call(bf16[256,1024]{1,0:T(8,128)(2,1)S(1)} %fusion.30.table_ref, f32[256,2048]{1,0:T(8,128)} %fusion.4.early_ref, bf16[1024,2048]{1,0:T(8,128)(2,1)} %bitcast.28.rows_ref), custom_call_target="tpu_custom_call" | custom-call | tf_op jit(solution)/shard_map/final_sum/pallas_call | solution.py:588
  (34 shorter events, 0.1 us)
Async XLA Ops:
  0.0 130.8 %copy-start = (bf16[1,512,2048]{2,1,0:T(8,128)(2,1)S(1)}, bf16[1,512,2048]{2,1,0:T(8,128)(2,1)}, u32[]{:S(2)}) copy-start(bf16[1,512,2048]{2,1,0:T(8,128)(2,1)} %param.36) | copy-start | bytes 6291460
  13.9 6.1 %collective-permute-start = (f32[128,256]{1,0:T(8,128)S(1)}, f32[128,256]{1,0:T(8,128)S(1)}, u32[]{:S(2)}, u32[]{:S(2)}) collective-permute-start(f32[128,256]{1,0:T(8,128)S(1)} %get-tuple-element.27), channel_id=1, source_target_pairs={{0,2},{2,4},{4,6},{6,0},{1,3},{3,5},{5,7},{7,1},{8,10},{10,12},{12... | collective-permute-start | bytes 393224 | tf_op jit(solution)/shard_map/ppermute | solution.py:292
  16.0 8.2 %collective-permute-start.1 = (f32[128,256]{1,0:T(8,128)S(1)}, f32[128,256]{1,0:T(8,128)S(1)}, u32[]{:S(2)}, u32[]{:S(2)}) collective-permute-start(f32[128,256]{1,0:T(8,128)S(1)} %get-tuple-element.28), channel_id=1, source_target_pairs={{0,4},{2,6},{4,0},{6,2},{1,5},{3,7},{5,1},{7,3},{8,12},{10,14},{12... | collective-permute-start | bytes 393224 | tf_op jit(solution)/shard_map/ppermute | solution.py:292
  18.4 5.7 %collective-permute-start.2 = (f32[128,256]{1,0:T(8,128)S(1)}, f32[128,256]{1,0:T(8,128)S(1)}, u32[]{:S(2)}, u32[]{:S(2)}) collective-permute-start(f32[128,256]{1,0:T(8,128)S(1)} %get-tuple-element.29), channel_id=1, source_target_pairs={{0,6},{2,0},{4,2},{6,4},{1,7},{3,1},{5,3},{7,5},{8,14},{10,8},{12,... | collective-permute-start | bytes 393224 | tf_op jit(solution)/shard_map/ppermute | solution.py:292
  24.8 5.2 %collective-permute-start.5 = (f32[128,256]{1,0:T(8,128)S(1)}, f32[128,256]{1,0:T(8,128)S(1)}, u32[]{:S(2)}, u32[]{:S(2)}) collective-permute-start(f32[128,256]{1,0:T(8,128)S(1)} %get-tuple-element.30.refs_0_), channel_id=1, source_target_pairs={{0,24},{8,0},{16,8},{24,16},{1,25},{9,1},{17,9},{25,17},{2,26},{10... | collective-permute-start | bytes 393224 | tf_op jit(solution)/shard_map/ppermute | solution.py:292
  27.6 5.4 %collective-permute-start.4 = (f32[128,256]{1,0:T(8,128)S(1)}, f32[128,256]{1,0:T(8,128)S(1)}, u32[]{:S(2)}, u32[]{:S(2)}) collective-permute-start(f32[128,256]{1,0:T(8,128)S(1)} %get-tuple-element.30.refs_0_), channel_id=1, source_target_pairs={{0,16},{8,24},{16,0},{24,8},{1,17},{9,25},{17,1},{25,9},{2,18},{10... | collective-permute-start | bytes 393224 | tf_op jit(solution)/shard_map/ppermute | solution.py:292
  27.9 8.5 %collective-permute-start.3 = (f32[128,256]{1,0:T(8,128)S(1)}, f32[128,256]{1,0:T(8,128)S(1)}, u32[]{:S(2)}, u32[]{:S(2)}) collective-permute-start(f32[128,256]{1,0:T(8,128)S(1)} %get-tuple-element.30.refs_0_), channel_id=1, source_target_pairs={{0,8},{8,16},{16,24},{24,0},{1,9},{9,17},{17,25},{25,1},{2,10},{10... | collective-permute-start | bytes 393224 | tf_op jit(solution)/shard_map/ppermute | solution.py:292
  37.0 9.5 %collective-permute-start.8 = (f32[128,256]{1,0:T(8,128)S(1)}, f32[128,256]{1,0:T(8,128)S(1)}, u32[]{:S(2)}, u32[]{:S(2)}) collective-permute-start(f32[128,256]{1,0:T(8,128)S(1)} %get-tuple-element.31), channel_id=1, source_target_pairs={{0,96},{1,97},{2,98},{3,99},{4,100},{5,101},{6,102},{7,103},{8,104... | collective-permute-start | bytes 393224 | tf_op jit(solution)/shard_map/ppermute | solution.py:297
  42.7 3.8 %collective-permute-start.7 = (f32[128,256]{1,0:T(8,128)S(1)}, f32[128,256]{1,0:T(8,128)S(1)}, u32[]{:S(2)}, u32[]{:S(2)}) collective-permute-start(f32[128,256]{1,0:T(8,128)S(1)} %get-tuple-element.31), channel_id=1, source_target_pairs={{0,64},{32,96},{1,65},{33,97},{2,66},{34,98},{3,67},{35,99},{4,68}... | collective-permute-start | bytes 393224 | tf_op jit(solution)/shard_map/ppermute | solution.py:297
  44.0 5.2 %collective-permute-start.6 = (f32[128,256]{1,0:T(8,128)S(1)}, f32[128,256]{1,0:T(8,128)S(1)}, u32[]{:S(2)}, u32[]{:S(2)}) collective-permute-start(f32[128,256]{1,0:T(8,128)S(1)} %get-tuple-element.31), channel_id=1, source_target_pairs={{0,32},{32,64},{64,96},{1,33},{33,65},{65,97},{2,34},{34,66},{66,9... | collective-permute-start | bytes 393224 | tf_op jit(solution)/shard_map/ppermute | solution.py:297
  49.2 11.1 %copy-start.5 = (f32[128]{0:T(128)S(1)}, f32[128]{0:T(128)}, u32[]{:S(2)}) copy-start(f32[128]{0:T(128)} %param.28) | copy-start | bytes 1540
  50.0 10.3 %collective-permute-start.9 = (f32[128,128]{1,0:T(8,128)S(1)}, f32[128,128]{1,0:T(8,128)S(1)}, u32[]{:S(2)}, u32[]{:S(2)}) collective-permute-start(f32[128,128]{1,0:T(8,128)S(1)} %get-tuple-element.35), channel_id=1, source_target_pairs={{0,6},{2,0},{4,2},{6,4},{1,7},{3,1},{5,3},{7,5},{8,14},{10,8},{12,... | collective-permute-start | bytes 196616 | tf_op jit(solution)/shard_map/ppermute | solution.py:292
  52.3 8.0 %collective-permute-start.10 = (f32[128,128]{1,0:T(8,128)S(1)}, f32[128,128]{1,0:T(8,128)S(1)}, u32[]{:S(2)}, u32[]{:S(2)}) collective-permute-start(f32[128,128]{1,0:T(8,128)S(1)} %get-tuple-element.36), channel_id=1, source_target_pairs={{0,4},{2,6},{4,0},{6,2},{1,5},{3,7},{5,1},{7,3},{8,12},{10,14},{12... | collective-permute-start | bytes 196616 | tf_op jit(solution)/shard_map/ppermute | solution.py:292
  53.2 7.1 %collective-permute-start.11 = (f32[128,128]{1,0:T(8,128)S(1)}, f32[128,128]{1,0:T(8,128)S(1)}, u32[]{:S(2)}, u32[]{:S(2)}) collective-permute-start(f32[128,128]{1,0:T(8,128)S(1)} %get-tuple-element.37), channel_id=1, source_target_pairs={{0,2},{2,4},{4,6},{6,0},{1,3},{3,5},{5,7},{7,1},{8,10},{10,12},{12... | collective-permute-start | bytes 196616 | tf_op jit(solution)/shard_map/ppermute | solution.py:292
  60.3 5.5 %copy-start.8 = (s32[256,4]{0,1:T(4,128)S(1)}, s32[256,4]{0,1:T(4,128)}, u32[]{:S(2)}) copy-start(s32[256,4]{0,1:T(4,128)} %param.32) | copy-start | bytes 12292
  60.3 6.7 %copy-start.4 = (f32[2048]{0:T(1024)S(1)}, f32[2048]{0:T(1024)}, u32[]{:S(2)}) copy-start(f32[2048]{0:T(1024)} %param.31) | copy-start | bytes 24580
  63.0 3.9 %collective-permute-start.12 = (bf16[256,512]{1,0:T(8,128)(2,1)S(1)}, bf16[256,512]{1,0:T(8,128)(2,1)S(1)}, u32[]{:S(2)}, u32[]{:S(2)}) collective-permute-start(bf16[256,512]{1,0:T(8,128)(2,1)S(1)} %get-tuple-element.43), channel_id=1, source_target_pairs={{0,1},{1,0},{2,3},{3,2},{4,5},{5,4},{6,7},{7,6},{8,9},{9,8},{10,11... | collective-permute-start | bytes 786440 | tf_op jit(solution)/shard_map/ppermute | solution.py:292
  66.0 7.6 %copy-start.2 = (f32[128,256]{1,0:T(8,128)}, f32[128,256]{1,0:T(8,128)S(1)}, u32[]{:S(2)}) copy-start(f32[128,256]{1,0:T(8,128)S(1)} %convolution_select_fusion.slot_ref) | copy-start | bytes 393220
  73.6 38.2 %all-to-all-start = ((bf16[128,8,1024]{2,1,0:T(8,128)(2,1)}), bf16[128,8,1024]{2,1,0:T(8,128)(2,1)}, u32[]{:S(2)}, u32[]{:S(2)}) async-start(bf16[128,8,1024]{2,1,0:T(8,128)(2,1)} %get-tuple-element.44), calls=%async_computation | async-start | bytes 4194304 | tf_op jit(solution)/shard_map/all_to_all | solution.py:398
  87.9 29.5 %copy-start.9 = (f32[256,4]{0,1:T(4,128)S(1)}, f32[256,4]{0,1:T(4,128)}, u32[]{:S(2)}) copy-start(f32[256,4]{0,1:T(4,128)} %param.33) | copy-start | bytes 12292
  87.9 30.5 %copy-start.3 = (f32[128,256]{1,0:T(8,128)S(1)}, f32[128,256]{1,0:T(8,128)}, u32[]{:S(2)}) copy-start(f32[128,256]{1,0:T(8,128)} %copy-done.2) | copy-start | bytes 393220
  111.8 58.2 %all-to-all-start.2 = ((bf16[128,8,2048]{2,1,0:T(8,128)(2,1)}), bf16[128,8,2048]{2,1,0:T(8,128)(2,1)}, u32[]{:S(2)}, u32[]{:S(2)}) async-start(bf16[128,8,2048]{2,1,0:T(8,128)(2,1)} %dispatch.1), calls=%async_computation.2 | async-start | bytes 8388608 | tf_op jit(solution)/shard_map/all_to_all | solution.py:398
  126.5 2.0 copy-start.10
  127.1 1.4 copy-start.6
  170.0 35.7 %all-to-all-start.1 = ((bf16[128,8,1024]{2,1,0:T(8,128)(2,1)}), bf16[128,8,1024]{2,1,0:T(8,128)(2,1)}, u32[]{:S(2)}, u32[]{:S(2)}) async-start(bf16[128,8,1024]{2,1,0:T(8,128)(2,1)} %reshape.230), calls=%async_computation.1 | async-start | bytes 4194304 | tf_op jit(solution)/shard_map/all_to_all | solution.py:398
  179.0 2.1 copy-start.11
  197.0 14.3 %copy-start.7 = (bf16[256,2048]{1,0:T(8,128)(2,1)S(1)}, bf16[256,2048]{1,0:T(8,128)(2,1)}, u32[]{:S(2)}) copy-start(bf16[256,2048]{1,0:T(8,128)(2,1)} %get-tuple-element.46.normed_ref) | copy-start | bytes 3145732
  205.8 58.2 %all-to-all-start.3 = ((bf16[128,8,2048]{2,1,0:T(8,128)(2,1)}), bf16[128,8,2048]{2,1,0:T(8,128)(2,1)}, u32[]{:S(2)}, u32[]{:S(2)}) async-start(bf16[128,8,2048]{2,1,0:T(8,128)(2,1)} %convert_bitcast_fusion), calls=%async_computation.3 | async-start | bytes 8388608 | tf_op jit(solution)/shard_map/all_to_all | solution.py:398
  217.1 3.6 %copy-start.12 = (bf16[256,2048]{1,0:T(8,128)(2,1)S(1)}, bf16[256,2048]{1,0:T(8,128)(2,1)}, u32[]{:S(2)}) copy-start(bf16[256,2048]{1,0:T(8,128)(2,1)} %get-tuple-element.45) | copy-start | bytes 3145732
  264.0 4.3 %copy-start.1 = (bf16[1,512,2048]{2,1,0:T(8,128)(2,1)S(1)}, bf16[1,512,2048]{2,1,0:T(8,128)(2,1)}, u32[]{:S(2)}) copy-start(bf16[1,512,2048]{2,1,0:T(8,128)(2,1)} %param.36) | copy-start | bytes 6291460
